TPU v7x, 256 devices: a whole 4x4x8 slice. The times are simulated.
256 devices in a mesh: sp: 64 (over z, y, core), tp: 4 (over x).
Axes of the slice: x: 4, y: 4, z: 8, core: 2. Of those that a mesh axis runs over, the one named last changes fastest.
Arguments:
- query_rows: bfloat16 [20480, 1024], P('sp', 'tp'), may hold values from -6 to 6
- key_rows: bfloat16 [20480, 1024], P('sp', 'tp'), may hold values from -6 to 6
- value_rows: bfloat16 [20480, 1024], P('sp', 'tp'), may hold values from -6 to 6
- key_shift: bfloat16 [20480, 16], P('sp', 'tp'), may hold values from -10 to 6
- documents: int32 [20480], P('sp'), may hold values from 0 to 31, never falling along the last dimension, each value on 1 to 1280 neighbouring positions
- out_weight: bfloat16 [1024, 2048], P('tp'), may hold values from -0.1875 to 0.1875
- stream: bfloat16 [20480, 2048], P('sp', 'tp'), may hold values from -8 to 8
- norm_gain: float32 [2048], replicated, may hold values from 0.1 to 1.9
- expert_ids: int32 [20480, 2], P('sp'), may hold values from 0 to 63, all different within a row; in each aligned block of 320 rows (0 to 319, 320 to 639, ...) at most 14 rows name the same one
- expert_weights: float32 [20480, 2], P('sp'), may hold values from 0.25 to 1
- gate_weight: bfloat16 [64, 2048, 3584], P('sp', None, 'tp'), may hold values from -0.125 to 0.125
- up_weight: bfloat16 [64, 2048, 3584], P('sp', None, 'tp'), may hold values from -0.125 to 0.125
- down_weight: bfloat16 [64, 3584, 2048], P('sp', 'tp'), may hold values from -0.09375 to 0.09375
Outputs:
- layer_out: bfloat16 [20480, 2048], P('sp', 'tp')
Inputs may be any that keep to these rules, and one draw needn't show every extreme that they name: `expert_ids`: in each aligned block of 320 rows no expert is named by more than 14 rows, a bound that some block reaches; the entries of a row differ. `documents`: document numbers never fall along the positions; each document has 1 to 1280 positions, and one has exactly 1280.
All inputs are finite; a program needn't handle non-finite values.
Results may differ from a plain program's by a relative error of at most 0.013.
Values may be sent and summed in bfloat16 or wider, within the bound.
No kernel may reach another device: no remote copies, remote signals or barrier semaphores. Data moves between devices by JAX's collectives and lax.ppermute only.
A program may use at most 128 MiB of HBM per device.

v0:
```python
import functools

import jax
import jax.numpy as jnp
from jax import lax
from jax.experimental import pallas as pl
from jax.experimental.pallas import tpu as pltpu
from jax.sharding import PartitionSpec as P


D = 2048
HEAD = 64
NORM_EPS = 1e-06
EXTRA = 16
LOG2E = 1.4426950408889634
F32 = jnp.float32
BF16 = jnp.bfloat16


def shifted(x, axis, by):
    size = lax.axis_size(axis)
    return lax.ppermute(x, axis, [(i, i + by) for i in range(size) if 0 <= i + by < size])


def rotated(x, axis, by):
    size = lax.axis_size(axis)
    return lax.ppermute(x, axis, [(i, (i + by) % size) for i in range(size)])


def attend_body(own, last, heads, *refs):
    if last:
        *refs, shift_scr, blk_scr, acc_ref, tot_ref = refs
        refs = (*refs, acc_ref, tot_ref)
    else:
        *refs, shift_scr, blk_scr = refs
    if own:
        q_ref, blk_ref, tri_ref, qdoc_ref, acc_ref, tot_ref = refs
    elif last:
        *refs, acc_ref, tot_ref = refs
        q_ref, near_ref, far_ref, tri_ref, qdoc_ref, acc_in, tot_in, done_ref = refs
    else:
        q_ref, near_ref, far_ref, tri_ref, qdoc_ref, acc_in, tot_in, acc_ref, tot_ref = refs
    rows = q_ref.shape[0]
    keys = shift_scr.shape[1]
    width = heads * HEAD
    groups = [(lo, min(keys, lo + 128)) for lo in range(0, keys, 128)]
    lane = lax.broadcasted_iota(jnp.int32, (rows, 128), 1)

    def one_head(blk, admitted, acc_old, tot_old, head):
        pair = head // 2
        cols = pl.ds(pl.multiple_of(128 * pair, 128), 128)
        v_cols = pl.ds(pl.multiple_of(width + 128 * pair, 128), 128)
        tot_cols = pl.ds(pl.multiple_of(128 * head, 128), 128)
        mine = (lane >= HEAD) == (head % 2 == 1)
        q_head = jnp.where(mine, q_ref[:, cols].astype(F32), 0.0).astype(BF16)
        later = None if tot_old is None else tot_old[:, tot_cols]
        shift = shift_scr[pl.ds(head, 1), :]
        scores = lax.dot_general(q_head, blk[0:keys, cols], (((1,), (1,)), ((), ())), preferred_element_type=F32)
        sticks = []
        for (lo, hi), ok in reversed(list(zip(groups, admitted))):
            size = hi - lo
            s = scores[:, lo:hi] * (LOG2E * HEAD ** (-0.5)) + shift[:, lo:hi]
            drop = jnp.maximum(s, 0.0) + jnp.log2(1.0 + jnp.exp2(-jnp.abs(s)))
            rest = jnp.where(ok, drop, 0.0)
            high = rest.astype(BF16)
            low = (rest - high.astype(F32)).astype(BF16)
            if size == 128:
                sums = jnp.dot(jnp.concatenate([high, low], axis=1), tri_ref[...], preferred_element_type=F32)
            else:
                sums = jnp.dot(high, tri_ref[0:size], preferred_element_type=F32) + jnp.dot(
                    low, tri_ref[0:size], preferred_element_type=F32
                )
            z = (s - drop) + sums[:, 0:size]
            if later is not None:
                z = z + later[:, 0:size]
            sticks.append(jnp.where(ok, jnp.exp2(z), 0.0).astype(BF16))
            gone = sums[:, 128:256]
            later = gone if later is None else later + gone
        stick = jnp.concatenate(sticks[::-1], axis=1)
        out = jnp.dot(stick, blk[0:keys, v_cols], preferred_element_type=F32)
        tot_ref[:, tot_cols] = later
        old = 0.0 if acc_old is None else acc_old[:, cols]
        acc_ref[:, cols] = old + jnp.where(mine, out, 0.0)

    def one_block(blk, acc_old, tot_old):
        extra = blk[keys : keys + EXTRA, 0:keys].astype(F32)
        shift_scr[...] = extra * LOG2E
        admitted = []
        for lo, hi in groups:
            ok = extra[heads : heads + 1, lo:hi] == qdoc_ref[...]
            if own:
                q_iota = lax.broadcasted_iota(jnp.int32, (rows, hi - lo), 0)
                k_iota = lax.broadcasted_iota(jnp.int32, (rows, hi - lo), 1) + lo
                ok = ok & (k_iota < q_iota)
            admitted.append(ok)
        lax.fori_loop(0, heads, lambda h, _: (one_head(blk, admitted, acc_old, tot_old, h), 0)[1], 0)

    if own:
        acc_ref[...] = jnp.zeros_like(acc_ref)
        one_block(blk_ref, acc_ref, None)
    else:
        acc_ref[...] = acc_in[...]
        tot_ref[...] = tot_in[...]

        def visit(t, _):
            @pl.when(t == 0)
            def _():
                blk_scr[...] = near_ref[...]

            @pl.when(t == 1)
            def _():
                blk_scr[...] = far_ref[...]

            one_block(blk_scr, acc_ref, tot_ref)
            return 0

        lax.fori_loop(0, 2, visit, 0)
        if last:
            done_ref[...] = acc_ref[...].astype(BF16)


def attend(own, last, heads, q, blks, tri, qdoc, state):
    rows = q.shape[0]
    outs = [
        jax.ShapeDtypeStruct((rows, heads * HEAD), F32),
        jax.ShapeDtypeStruct((rows, heads * 128), F32),
    ]
    scratch = []
    if last:
        scratch = [pltpu.VMEM(o.shape, o.dtype) for o in outs]
        outs = [jax.ShapeDtypeStruct((rows, heads * HEAD), BF16)]
    keys = blks[0].shape[0] - EXTRA
    return pl.pallas_call(
        functools.partial(attend_body, own, last, heads),
        out_shape=outs,
        scratch_shapes=[pltpu.VMEM((EXTRA, keys), F32), pltpu.VMEM(blks[0].shape, BF16)] + scratch,
        name="attend_own" if own else "attend_visit",
        cost_estimate=pl.CostEstimate(
            flops=len(blks) * 2 * heads * rows * keys * (2 * HEAD + 2 * keys),
            transcendentals=len(blks) * 3 * heads * rows * keys,
            bytes_accessed=2 * blks[0].size * len(blks) + 4 * rows * heads * HEAD,
        ),
        compiler_params=pltpu.CompilerParams(vmem_limit_bytes=24 << 20),
    )(q, *blks, tri, qdoc, *state)


def expert_body(
    take_ref, own, left, right, opp_t, opp_b, gain, gate_w, up_w, down_w,
    out_ft, out_fb, out_up, out_down, out_own, norm, g_acc, hid, gate_v, up_v, down_v, sems,
):
    half = opp_t.shape[0]
    cols = own.shape[1]

    def fetches(i):
        rows = pl.ds(pl.multiple_of(take_ref[i] * cols, cols), cols)
        lanes = pl.ds(pl.multiple_of(take_ref[4 + i] * cols, cols), cols)
        return (
            pltpu.make_async_copy(gate_w.at[0, rows], gate_v.at[i], sems.at[0, i]),
            pltpu.make_async_copy(up_w.at[0, rows], up_v.at[i], sems.at[1, i]),
            pltpu.make_async_copy(down_w.at[0, :, lanes], down_v.at[i], sems.at[2, i]),
        )

    for kind in range(3):
        for i in range(4):
            fetches(i)[kind].start()

    def whole(kind):
        for i in range(4):
            fetches(i)[kind].wait()

    for base, opp in ((0, opp_t), (half, opp_b)):

        def normed(t, _, base=base, opp=opp):
            here = pl.ds(pl.multiple_of(base + 32 * t, 32), 32)
            there = pl.ds(pl.multiple_of(32 * t, 32), 32)
            wide = [r.astype(F32) for r in (own[here], left[here], right[here], opp[there])]
            total = sum(jnp.sum(w * w, axis=1, keepdims=True) for w in wide)
            inv = lax.rsqrt(total / D + NORM_EPS)
            for i in range(4):
                norm[i, here] = (wide[i] * inv * gain[take_ref[i]]).astype(BF16)
            return 0

        lax.fori_loop(0, half // 32, normed, 0)
    whole(0)
    g_acc[...] = sum(jnp.dot(norm[i], gate_v[i], preferred_element_type=F32) for i in range(4))
    whole(1)
    u = sum(jnp.dot(norm[i], up_v[i], preferred_element_type=F32) for i in range(4))
    g = g_acc[...]
    hid[...] = (g / (1.0 + jnp.exp(-g)) * u).astype(BF16)
    whole(2)

    def down(i, _):
        norm[i] = jnp.dot(hid[...], down_v[i], preferred_element_type=F32).astype(BF16)
        return 0

    lax.fori_loop(0, 4, down, 0)
    out_ft[...] = norm[0, :half]
    out_fb[...] = norm[0, half:]
    out_up[...] = norm[1]
    out_down[...] = norm[2]
    out_own[...] = norm[3]


def experts_of(take, own, left, right, opp_t, opp_b, gain, gate_w, up_w, down_w):
    rows, cols = own.shape
    hidden = gate_w.shape[2]
    smem = pl.BlockSpec(memory_space=pltpu.SMEM)
    vmem = pl.BlockSpec(memory_space=pltpu.VMEM)
    hbm = pl.BlockSpec(memory_space=pltpu.HBM)
    shape = lambda r: jax.ShapeDtypeStruct((r, cols), BF16)
    return pl.pallas_call(
        expert_body,
        out_shape=[shape(rows // 2), shape(rows // 2), shape(rows), shape(rows), shape(rows)],
        in_specs=[smem] + [vmem] * 6 + [hbm] * 3,
        out_specs=[vmem] * 5,
        scratch_shapes=[
            pltpu.VMEM((4, rows, cols), BF16),
            pltpu.VMEM((rows, hidden), F32),
            pltpu.VMEM((rows, hidden), BF16),
            pltpu.VMEM((4, cols, hidden), BF16),
            pltpu.VMEM((4, cols, hidden), BF16),
            pltpu.VMEM((4, hidden, cols), BF16),
            pltpu.SemaphoreType.DMA((3, 4)),
        ],
        name="experts",
        cost_estimate=pl.CostEstimate(
            flops=6 * rows * 4 * cols * hidden,
            transcendentals=rows * hidden,
            bytes_accessed=2 * 12 * cols * hidden + 16 * rows * cols,
        ),
        compiler_params=pltpu.CompilerParams(vmem_limit_bytes=48 << 20),
    )(take, own, left, right, opp_t, opp_b, gain, gate_w, up_w, down_w)


def gather_tp(x):
    half = x.shape[0] // 2
    left = rotated(x, "tp", 1)
    right = rotated(x, "tp", -1)
    opp_t = rotated(left[:half], "tp", 1)
    opp_b = rotated(right[half:], "tp", -1)
    return left, right, opp_t, opp_b


def scatter_sum_tp(parts, shape):
    far_t, far_b, up, down, own = parts
    half = far_t.shape[0]
    from_left = rotated(far_t, "tp", 1)
    from_right = rotated(far_b, "tp", -1)
    add = lambda a, b: (a.astype(F32) + b.astype(F32)).astype(BF16)
    up = lax.dynamic_update_slice(up, add(up[:half], from_left), (0, 0))
    down = lax.dynamic_update_slice(down, add(down[half:], from_right), (half, 0))
    a = rotated(up, "tp", 1)
    b = rotated(down, "tp", -1)
    return (own.astype(F32) + a.astype(F32) + b.astype(F32)).astype(BF16).reshape(shape)


def layer(
    query_rows,
    key_rows,
    value_rows,
    key_shift,
    documents,
    out_weight,
    stream,
    norm_gain,
    expert_ids,
    expert_weights,
    gate_weight,
    up_weight,
    down_weight,
):
    rows, width = query_rows.shape
    heads = key_shift.shape[1]
    cols = stream.shape[1]
    me = lax.axis_index("tp")

    doc = (documents + 1).astype(F32)
    extra = jnp.concatenate(
        [jnp.transpose(key_shift), doc[None].astype(BF16), jnp.zeros((EXTRA - heads - 1, rows), BF16)], axis=0
    )
    extra = jnp.pad(extra, ((0, 0), (0, 2 * width - rows)))
    packed = jnp.concatenate([jnp.concatenate([key_rows, value_rows], axis=1), extra], axis=0)
    odd = lax.rem(lax.axis_index("sp"), 2) == 1
    size = lax.axis_size("sp")
    swap = lambda x: lax.ppermute(x, "sp", [(i, i ^ 1) for i in range(size)])
    two = shifted(packed, "sp", 2)
    four = shifted(two, "sp", 2)
    one = swap(jnp.where(odd, two, packed))
    held = lax.optimization_barrier((two, one))[0]
    three = swap(jnp.where(odd, four, held))

    cut = lambda k: lax.dynamic_slice_in_dim(out_weight, lax.rem(me + k, 4) * cols, cols, axis=1)
    w_own = cut(0)
    w_left = rotated(cut(1), "tp", 1)
    w_right = rotated(cut(3), "tp", -1)
    w_opp = rotated(cut(2), "tp", 2)

    qdoc = doc[:, None]
    iota = jnp.arange(rows, dtype=jnp.int32)
    later = (iota[:, None] > iota[None, :]).astype(BF16)
    lanes = jnp.arange(128, dtype=jnp.int32)
    tri = jnp.where(lanes[:, None] > lanes[None, :], -1.0, 0.0)
    tri = jnp.concatenate([tri, jnp.full((128, 128), -1.0)], axis=1).astype(BF16)
    tri = jnp.concatenate([tri, tri], axis=0)
    state = attend(True, False, heads, query_rows, (packed,), tri, qdoc, ())
    state = attend(False, False, heads, query_rows, (one, two), tri, qdoc, state)
    state = attend(False, True, heads, query_rows, (three, four), tri, qdoc, state)
    attended = state[0]

    top = expert_ids.shape[1]
    experts = size * gate_weight.shape[0]
    capacity = (4 * rows * top + 3 * experts - 1) // (3 * experts)
    e_iota = jnp.arange(experts, dtype=jnp.int32)[None, :]
    chosen = [(expert_ids[:, k : k + 1] == e_iota) for k in range(top)]
    count = sum(c.astype(BF16) for c in chosen)
    earlier = jnp.dot(later, count, preferred_element_type=F32)
    ids = [expert_ids[:, k : k + 1] for k in range(top)]
    slot = [jnp.sum(jnp.where(c, earlier, 0.0), axis=1, keepdims=True).astype(jnp.int32) for c in chosen]
    targets = jnp.arange(experts * capacity, dtype=jnp.int32)[None]
    select = sum((i * capacity + s == targets).astype(BF16) for i, s in zip(ids, slot))

    left, right, opp_t, opp_b = gather_tp(attended)
    opp = jnp.concatenate([opp_t, opp_b], axis=0)
    part = lambda a, w: jnp.dot(a, w, preferred_element_type=F32).astype(BF16).astype(F32)
    projected = part(attended, w_own) + part(left, w_left) + part(right, w_right) + part(opp, w_opp)
    middle = (stream.astype(F32) + projected).astype(BF16)

    send = lax.dot_general(select, middle, (((0,), (0,)), ((), ())), preferred_element_type=F32)
    send = send.astype(BF16).reshape(experts, capacity, cols)
    block = lax.all_to_all(send, "sp", 0, 0, tiled=True)
    take = lax.rem(jnp.array([0, 3, 1, 2, 2, 1, 3, 0], jnp.int32) + me, 4)
    gain = norm_gain.reshape(4, 1, cols)
    mixed = middle.astype(F32)
    for lo, hi in ((8, capacity), (0, 8)):
        items = hi - lo
        part = block[:, lo:hi].reshape(experts * items, cols)
        wide = gather_tp(part)
        parts = experts_of(take, part, *wide, gain, gate_weight, up_weight, down_weight)
        result = scatter_sum_tp(parts, (experts, items, cols))
        back = lax.all_to_all(result, "sp", 0, 0, tiled=True).reshape(experts * items, cols)

        slots = jnp.arange(experts * items, dtype=jnp.int32)[None]
        for k in range(top):
            place = jnp.where((slot[k] >= lo) & (slot[k] < hi), ids[k] * items + slot[k] - lo, -1)
            value = jnp.dot((place == slots).astype(BF16), back, preferred_element_type=F32)
            mixed = mixed + value * expert_weights[:, k : k + 1]
    return mixed.astype(BF16)


def solution(mesh):
    in_specs = (
        P("sp", "tp"),
        P("sp", "tp"),
        P("sp", "tp"),
        P("sp", "tp"),
        P("sp"),
        P("tp", None),
        P("sp", "tp"),
        P(),
        P("sp", None),
        P("sp", None),
        P("sp", None, "tp"),
        P("sp", None, "tp"),
        P("sp", "tp", None),
    )
    out_specs = P("sp", "tp")
    return jax.shard_map(layer, mesh=mesh, in_specs=in_specs, out_specs=out_specs, check_vma=False)
```

profile of v0, /device:TPU:1, one launch (start us, length us, event | category | flops | bytes accessed | tf_op | source)
XLA Modules:
  0.0 228.1 jit_solution(1935435943848528034)
XLA Ops:
  3.2 4.0 %collective-permute-start = (bf16[336,512]{1,0:T(8,128)(2,1)S(1)}, bf16[336,512]{1,0:T(8,128)(2,1)S(1)}, u32[]{:S(2)}, u32[]{:S(2)}) collective-permute-start(bf16[336,512]{1,0:T(8,128)(2,1)S(1)} %fusion.26.refs_1_), channel_id=1, source_target_pairs={{0,8},{4,12},{8,16},{12,20},{16,24},{20,28},{24,32},{28,36},{32,40... | collective-permute-start | bytes 1032200 | tf_op jit(solution)/shard_map/ppermute | solution.py:22
  7.3 6.7 %collective-permute-done.refs_2_ = bf16[336,512]{1,0:T(8,128)(2,1)S(1)} collective-permute-done((bf16[336,512]{1,0:T(8,128)(2,1)S(1)}, bf16[336,512]{1,0:T(8,128)(2,1)S(1)}, u32[]{:S(2)}, u32[]{:S(2)}) %collective-permute-start) | collective-permute-done | bytes 344096 | tf_op jit(solution)/shard_map/ppermute | solution.py:22
  15.1 1.6 collective-permute-start.2
  16.7 4.1 %collective-permute-start.1 = (bf16[336,512]{1,0:T(8,128)(2,1)S(1)}, bf16[336,512]{1,0:T(8,128)(2,1)S(1)}, u32[]{:S(2)}, u32[]{:S(2)}) collective-permute-start(bf16[336,512]{1,0:T(8,128)(2,1)S(1)} %collective-permute-done.refs_2_), channel_id=1, source_target_pairs={{0,8},{4,12},{8,16},{12,20},{16,24},{20,28},{24,32},{28,36},{32,40... | collective-permute-start | bytes 1032200 | tf_op jit(solution)/shard_map/ppermute | solution.py:22
  22.2 2.5 %collective-permute-start.10 = (bf16[256,512]{1,0:T(8,128)(2,1)S(1)}, bf16[256,512]{1,0:T(8,128)(2,1)}, u32[]{:S(2)}, u32[]{:S(2)}) collective-permute-start(bf16[256,512]{1,0:T(8,128)(2,1)S(1)} %get-tuple-element.51), channel_id=1, source_target_pairs={{0,2},{1,3},{2,0},{3,1},{4,6},{5,7},{6,4},{7,5},{8,10},{9,11},{10,... | collective-permute-start | bytes 786440 | tf_op jit(solution)/shard_map/ppermute | solution.py:27
  25.9 2.3 collective-permute-done.1.refs_2_
  29.3 2.9 %attend_own.1 = (f32[320,256]{1,0:T(8,128)S(1)}, f32[320,512]{1,0:T(8,128)S(1)}) custom-call(bf16[320,256]{1,0:T(8,128)(2,1)S(1)} %copy-done, bf16[336,512]{1,0:T(8,128)(2,1)S(1)} %fusion.26.refs_1_, bf16[256,256]{1,0:T(8,128)(2,1)S(1)} %pad_maximum_fusion.refs_2_.refs_3_, f32[320,1]{1,0:T(8,128)S(1)} %broadcast_in_dim.44.refs_3_.refs_4_), custom_call_target="tpu_custom_call" | custom-call | flops 629145600 | bytes 671744 | tf_op jit(solution)/shard_map/attend_own/pallas_call | solution.py:133
  32.3 6.1 %attend_visit.2 = (f32[320,256]{1,0:T(8,128)S(1)}, f32[320,512]{1,0:T(8,128)S(1)}) custom-call(bf16[320,256]{1,0:T(8,128)(2,1)S(1)} %copy-done, bf16[336,512]{1,0:T(8,128)(2,1)S(1)} %collective-permute-done.2.refs_1_, bf16[336,512]{1,0:T(8,128)(2,1)S(1)} %collective-permute-done.refs_2_, bf16[256,256]{1,0:T(8,128)(2,1)S(1)} %pad_maximum_fusion.refs_2_.refs_3_, ...), custom_call_target="tpu_custom_call" | custom-call | flops 1258291200 | bytes 1015808 | tf_op jit(solution)/shard_map/attend_visit/pallas_call | solution.py:133
  38.4 6.1 %attend_visit.3 = bf16[320,256]{1,0:T(8,128)(2,1)S(1)} custom-call(bf16[320,256]{1,0:T(8,128)(2,1)S(1)} %copy-done, bf16[336,512]{1,0:T(8,128)(2,1)S(1)} %collective-permute-done.3.refs_1_, bf16[336,512]{1,0:T(8,128)(2,1)S(1)} %collective-permute-done.1.refs_2_, bf16[256,256]{1,0:T(8,128)(2,1)S(1)} %pad_maximum_fusion.refs_2_.refs_3_, ...), custom_call_target="tpu_custom_call" | custom-call | flops 1258291200 | bytes 1015808 | tf_op jit(solution)/shard_map/attend_visit/pallas_call | solution.py:133
  44.5 2.6 %collective-permute-start.6 = (bf16[320,256]{1,0:T(8,128)(2,1)S(1)}, bf16[320,256]{1,0:T(8,128)(2,1)S(1)}, u32[]{:S(2)}, u32[]{:S(2)}) collective-permute-start(bf16[320,256]{1,0:T(8,128)(2,1)S(1)} %attend_visit.3), channel_id=1, source_target_pairs={{0,3},{1,0},{2,1},{3,2},{4,7},{5,4},{6,5},{7,6},{8,11},{9,8},{10,9... | collective-permute-start | bytes 491528 | tf_op jit(solution)/shard_map/ppermute | solution.py:27
  47.9 2.6 %collective-permute-done.6 = bf16[320,256]{1,0:T(8,128)(2,1)S(1)} collective-permute-done((bf16[320,256]{1,0:T(8,128)(2,1)S(1)}, bf16[320,256]{1,0:T(8,128)(2,1)S(1)}, u32[]{:S(2)}, u32[]{:S(2)}) %collective-permute-start.6) | collective-permute-done | bytes 163872 | tf_op jit(solution)/shard_map/ppermute | solution.py:27
  50.6 3.4 %collective-permute-start.9 = (bf16[160,256]{1,0:T(8,128)(2,1)S(1)}, bf16[160,256]{1,0:T(8,128)(2,1)S(1)}, u32[]{:S(2)}, u32[]{:S(2)}) collective-permute-start(bf16[160,256]{1,0:T(8,128)(2,1)S(1)} %slice.69), channel_id=1, source_target_pairs={{0,3},{1,0},{2,1},{3,2},{4,7},{5,4},{6,5},{7,6},{8,11},{9,8},{10,9... | collective-permute-start | bytes 245768 | tf_op jit(solution)/shard_map/ppermute | solution.py:27
  56.6 2.0 collective-permute-done.8
  61.2 46.9 %all_to_all.15 = bf16[64,14,512]{2,1,0:T(8,128)(2,1)S(1)} all-to-all(bf16[64,14,512]{2,1,0:T(8,128)(2,1)S(1)} %reshape.107), channel_id=1, replica_groups=mesh['sp'=64,'tp'=4] {'sp'}, dimensions={0} | all-to-all | bytes 1835008 | tf_op jit(solution)/shard_map/all_to_all | solution.py:330
  111.4 6.5 %collective-permute-done.12.right = bf16[384,512]{1,0:T(8,128)(2,1)S(1)} collective-permute-done((bf16[384,512]{1,0:T(8,128)(2,1)S(1)}, bf16[384,512]{1,0:T(8,128)(2,1)S(1)}, u32[]{:S(2)}, u32[]{:S(2)}) %collective-permute-start.12) | collective-permute-done | bytes 393248 | tf_op jit(solution)/shard_map/ppermute | solution.py:27
  117.8 1.5 collective-permute-start.14
  119.5 9.6 %collective-permute-done.20.right = bf16[512,512]{1,0:T(8,128)(2,1)S(1)} collective-permute-done((bf16[512,512]{1,0:T(8,128)(2,1)S(1)}, bf16[512,512]{1,0:T(8,128)(2,1)S(1)}, u32[]{:S(2)}, u32[]{:S(2)}) %collective-permute-start.20) | collective-permute-done | bytes 524320 | tf_op jit(solution)/shard_map/ppermute | solution.py:27
  129.1 1.5 collective-permute-start.22
  130.7 2.5 %collective-permute-done.14.opp_b = bf16[192,512]{1,0:T(8,128)(2,1)S(1)} collective-permute-done((bf16[192,512]{1,0:T(8,128)(2,1)S(1)}, bf16[192,512]{1,0:T(8,128)(2,1)S(1)}, u32[]{:S(2)}, u32[]{:S(2)}) %collective-permute-start.14) | collective-permute-done | bytes 196640 | tf_op jit(solution)/shard_map/ppermute | solution.py:27
  134.6 8.7 %experts.2 = (bf16[192,512]{1,0:T(8,128)(2,1)S(1)}, bf16[192,512]{1,0:T(8,128)(2,1)S(1)}, bf16[384,512]{1,0:T(8,128)(2,1)S(1)}, bf16[384,512]{1,0:T(8,128)(2,1)S(1)}, bf16[384,512]{1,0:T(8,128)(2,1)S(1)}) custom-call(s32[8]{0:T(128)S(1)} %compare_select_fusion.take_ref, bf16[384,512]{1,0:T(8,128)(2,1)S(1)} %reshape.108.own, ...), custom_call_target="tpu_custom_call" | custom-call | flops 4227858432 | bytes 14155776 | tf_op jit(solution)/shard_map/experts/pallas_call | solution.py:211
  143.3 2.7 %collective-permute-start.17 = (bf16[192,512]{1,0:T(8,128)(2,1)S(1)}, bf16[192,512]{1,0:T(8,128)(2,1)S(1)}, u32[]{:S(2)}, u32[]{:S(2)}) collective-permute-start(bf16[192,512]{1,0:T(8,128)(2,1)S(1)} %get-tuple-element.29), channel_id=1, source_target_pairs={{0,3},{1,0},{2,1},{3,2},{4,7},{5,4},{6,5},{7,6},{8,11},{9,8},{10,9... | collective-permute-start | bytes 589832 | tf_op jit(solution)/shard_map/ppermute | solution.py:27
  146.0 10.4 %experts.3 = (bf16[256,512]{1,0:T(8,128)(2,1)S(1)}, bf16[256,512]{1,0:T(8,128)(2,1)S(1)}, bf16[512,512]{1,0:T(8,128)(2,1)S(1)}, bf16[512,512]{1,0:T(8,128)(2,1)S(1)}, bf16[512,512]{1,0:T(8,128)(2,1)S(1)}) custom-call(s32[8]{0:T(128)S(1)} %compare_select_fusion.take_ref, bf16[512,512]{1,0:T(8,128)(2,1)S(1)} %slice_bitcast_fusion.own, ...), custom_call_target="tpu_custom_call" | custom-call | flops 5637144576 | bytes 15204352 | tf_op jit(solution)/shard_map/experts/pallas_call | solution.py:211
  156.5 2.7 %collective-permute-start.25 = (bf16[256,512]{1,0:T(8,128)(2,1)S(1)}, bf16[256,512]{1,0:T(8,128)(2,1)S(1)}, u32[]{:S(2)}, u32[]{:S(2)}) collective-permute-start(bf16[256,512]{1,0:T(8,128)(2,1)S(1)} %get-tuple-element.34), channel_id=1, source_target_pairs={{0,3},{1,0},{2,1},{3,2},{4,7},{5,4},{6,5},{7,6},{8,11},{9,8},{10,9... | collective-permute-start | bytes 786440 | tf_op jit(solution)/shard_map/ppermute | solution.py:27
  159.4 1.5 collective-permute-start.16
  161.0 1.6 collective-permute-done.25
  162.6 3.2 %collective-permute-start.26 = (bf16[512,512]{1,0:T(8,128)(2,1)S(1)}, bf16[512,512]{1,0:T(8,128)(2,1)S(1)}, u32[]{:S(2)}, u32[]{:S(2)}) collective-permute-start(bf16[512,512]{1,0:T(8,128)(2,1)S(1)} %fusion.30), channel_id=1, source_target_pairs={{0,3},{1,0},{2,1},{3,2},{4,7},{5,4},{6,5},{7,6},{8,11},{9,8},{10,9... | collective-permute-start | bytes 1572872 | tf_op jit(solution)/shard_map/ppermute | solution.py:27
  166.0 2.9 %collective-permute-done.18 = bf16[384,512]{1,0:T(8,128)(2,1)S(1)} collective-permute-done((bf16[384,512]{1,0:T(8,128)(2,1)S(1)}, bf16[384,512]{1,0:T(8,128)(2,1)S(1)}, u32[]{:S(2)}, u32[]{:S(2)}) %collective-permute-start.18) | collective-permute-done | bytes 393248 | tf_op jit(solution)/shard_map/ppermute | solution.py:27
  171.4 14.1 %all-to-all-start.1 = ((bf16[64,6,512]{2,1,0:T(8,128)(2,1)}), bf16[64,6,512]{2,1,0:T(8,128)(2,1)S(1)}, u32[]{:S(2)}, u32[]{:S(2)}) async-start(bf16[64,6,512]{2,1,0:T(8,128)(2,1)} %reshape.110), calls=%async_computation.1 | async-start | bytes 1048576 | tf_op jit(solution)/shard_map/all_to_all | solution.py:340
  185.5 2.0 fusion.22
  187.5 15.6 %all-to-all-done.1 = bf16[64,6,512]{2,1,0:T(8,128)(2,1)S(1)} async-done(((bf16[64,6,512]{2,1,0:T(8,128)(2,1)}), bf16[64,6,512]{2,1,0:T(8,128)(2,1)S(1)}, u32[]{:S(2)}, u32[]{:S(2)}) %all-to-all-start.1) | async-done | bytes 393248 | tf_op jit(solution)/shard_map/all_to_all | solution.py:340
  203.2 5.7 %all-to-all-start.2 = ((bf16[64,8,512]{2,1,0:T(8,128)(2,1)}), bf16[64,8,512]{2,1,0:T(8,128)(2,1)S(1)}, u32[]{:S(2)}, u32[]{:S(2)}) async-start(bf16[64,8,512]{2,1,0:T(8,128)(2,1)} %fusion.22), calls=%async_computation.2 | async-start | bytes 1048576 | tf_op jit(solution)/shard_map/all_to_all | solution.py:340
  210.0 16.6 %all-to-all-done.2 = bf16[64,8,512]{2,1,0:T(8,128)(2,1)S(1)} async-done(((bf16[64,8,512]{2,1,0:T(8,128)(2,1)}), bf16[64,8,512]{2,1,0:T(8,128)(2,1)S(1)}, u32[]{:S(2)}, u32[]{:S(2)}) %all-to-all-start.2) | async-done | bytes 524320 | tf_op jit(solution)/shard_map/all_to_all | solution.py:340
  (103 shorter events, 24.5 us)
Async XLA Ops:
  3.2 10.8 %collective-permute-start = (bf16[336,512]{1,0:T(8,128)(2,1)S(1)}, bf16[336,512]{1,0:T(8,128)(2,1)S(1)}, u32[]{:S(2)}, u32[]{:S(2)}) collective-permute-start(bf16[336,512]{1,0:T(8,128)(2,1)S(1)} %fusion.26.refs_1_), channel_id=1, source_target_pairs={{0,8},{4,12},{8,16},{12,20},{16,24},{20,28},{24,32},{28,36},{32,40... | collective-permute-start | bytes 1032200 | tf_op jit(solution)/shard_map/ppermute | solution.py:22
  15.1 10.8 %collective-permute-start.2 = (bf16[336,512]{1,0:T(8,128)(2,1)S(1)}, bf16[336,512]{1,0:T(8,128)(2,1)S(1)}, u32[]{:S(2)}, u32[]{:S(2)}) collective-permute-start(bf16[336,512]{1,0:T(8,128)(2,1)S(1)} %broadcast_select_fusion.1), channel_id=1, source_target_pairs={{0,4},{4,0},{8,12},{12,8},{16,20},{20,16},{24,28},{28,24},{32,36},... | collective-permute-start | bytes 1032200 | tf_op jit(solution)/shard_map/ppermute | solution.py:285
  16.7 11.5 %collective-permute-start.1 = (bf16[336,512]{1,0:T(8,128)(2,1)S(1)}, bf16[336,512]{1,0:T(8,128)(2,1)S(1)}, u32[]{:S(2)}, u32[]{:S(2)}) collective-permute-start(bf16[336,512]{1,0:T(8,128)(2,1)S(1)} %collective-permute-done.refs_2_), channel_id=1, source_target_pairs={{0,8},{4,12},{8,16},{12,20},{16,24},{20,28},{24,32},{28,36},{32,40... | collective-permute-start | bytes 1032200 | tf_op jit(solution)/shard_map/ppermute | solution.py:22
  20.9 33.2 %collective-permute-start.5 = (bf16[256,512]{1,0:T(8,128)(2,1)S(1)}, bf16[256,512]{1,0:T(8,128)(2,1)}, u32[]{:S(2)}, u32[]{:S(2)}) collective-permute-start(bf16[256,512]{1,0:T(8,128)(2,1)S(1)} %get-tuple-element.50), channel_id=1, source_target_pairs={{0,1},{1,2},{2,3},{3,0},{4,5},{5,6},{6,7},{7,4},{8,9},{9,10},{10,1... | collective-permute-start | bytes 786440 | tf_op jit(solution)/shard_map/ppermute | solution.py:27
  22.2 34.3 %collective-permute-start.10 = (bf16[256,512]{1,0:T(8,128)(2,1)S(1)}, bf16[256,512]{1,0:T(8,128)(2,1)}, u32[]{:S(2)}, u32[]{:S(2)}) collective-permute-start(bf16[256,512]{1,0:T(8,128)(2,1)S(1)} %get-tuple-element.51), channel_id=1, source_target_pairs={{0,2},{1,3},{2,0},{3,1},{4,6},{5,7},{6,4},{7,5},{8,10},{9,11},{10,... | collective-permute-start | bytes 786440 | tf_op jit(solution)/shard_map/ppermute | solution.py:27
  24.7 30.6 %collective-permute-start.7 = (bf16[256,512]{1,0:T(8,128)(2,1)S(1)}, bf16[256,512]{1,0:T(8,128)(2,1)}, u32[]{:S(2)}, u32[]{:S(2)}) collective-permute-start(bf16[256,512]{1,0:T(8,128)(2,1)S(1)} %get-tuple-element.52), channel_id=1, source_target_pairs={{0,3},{1,0},{2,1},{3,2},{4,7},{5,4},{6,5},{7,6},{8,11},{9,8},{10,9... | collective-permute-start | bytes 786440 | tf_op jit(solution)/shard_map/ppermute | solution.py:27
  28.2 10.2 %collective-permute-start.3 = (bf16[336,512]{1,0:T(8,128)(2,1)S(1)}, bf16[336,512]{1,0:T(8,128)(2,1)S(1)}, u32[]{:S(2)}, u32[]{:S(2)}) collective-permute-start(bf16[336,512]{1,0:T(8,128)(2,1)S(1)} %broadcast_select_fusion), channel_id=1, source_target_pairs={{0,4},{4,0},{8,12},{12,8},{16,20},{20,16},{24,28},{28,24},{32,36},... | collective-permute-start | bytes 1032200 | tf_op jit(solution)/shard_map/ppermute | solution.py:285
  44.5 6.1 %collective-permute-start.6 = (bf16[320,256]{1,0:T(8,128)(2,1)S(1)}, bf16[320,256]{1,0:T(8,128)(2,1)S(1)}, u32[]{:S(2)}, u32[]{:S(2)}) collective-permute-start(bf16[320,256]{1,0:T(8,128)(2,1)S(1)} %attend_visit.3), channel_id=1, source_target_pairs={{0,3},{1,0},{2,1},{3,2},{4,7},{5,4},{6,5},{7,6},{8,11},{9,8},{10,9... | collective-permute-start | bytes 491528 | tf_op jit(solution)/shard_map/ppermute | solution.py:27
  47.0 7.0 %collective-permute-start.4 = (bf16[320,256]{1,0:T(8,128)(2,1)S(1)}, bf16[320,256]{1,0:T(8,128)(2,1)S(1)}, u32[]{:S(2)}, u32[]{:S(2)}) collective-permute-start(bf16[320,256]{1,0:T(8,128)(2,1)S(1)} %attend_visit.3), channel_id=1, source_target_pairs={{0,1},{1,2},{2,3},{3,0},{4,5},{5,6},{6,7},{7,4},{8,9},{9,10},{10,1... | collective-permute-start | bytes 491528 | tf_op jit(solution)/shard_map/ppermute | solution.py:27
  50.6 6.0 %collective-permute-start.9 = (bf16[160,256]{1,0:T(8,128)(2,1)S(1)}, bf16[160,256]{1,0:T(8,128)(2,1)S(1)}, u32[]{:S(2)}, u32[]{:S(2)}) collective-permute-start(bf16[160,256]{1,0:T(8,128)(2,1)S(1)} %slice.69), channel_id=1, source_target_pairs={{0,3},{1,0},{2,1},{3,2},{4,7},{5,4},{6,5},{7,6},{8,11},{9,8},{10,9... | collective-permute-start | bytes 245768 | tf_op jit(solution)/shard_map/ppermute | solution.py:27
  54.0 4.6 %collective-permute-start.8 = (bf16[160,256]{1,0:T(8,128)(2,1)S(1)}, bf16[160,256]{1,0:T(8,128)(2,1)S(1)}, u32[]{:S(2)}, u32[]{:S(2)}) collective-permute-start(bf16[160,256]{1,0:T(8,128)(2,1)S(1)} %slice.68), channel_id=1, source_target_pairs={{0,1},{1,2},{2,3},{3,0},{4,5},{5,6},{6,7},{7,4},{8,9},{9,10},{10,1... | collective-permute-start | bytes 245768 | tf_op jit(solution)/shard_map/ppermute | solution.py:27
  108.2 9.6 %collective-permute-start.12 = (bf16[384,512]{1,0:T(8,128)(2,1)S(1)}, bf16[384,512]{1,0:T(8,128)(2,1)S(1)}, u32[]{:S(2)}, u32[]{:S(2)}) collective-permute-start(bf16[384,512]{1,0:T(8,128)(2,1)S(1)} %reshape.108.own), channel_id=1, source_target_pairs={{0,3},{1,0},{2,1},{3,2},{4,7},{5,4},{6,5},{7,6},{8,11},{9,8},{10,9... | collective-permute-start | bytes 1179656 | tf_op jit(solution)/shard_map/ppermute | solution.py:27
  108.3 11.0 %collective-permute-start.11 = (bf16[384,512]{1,0:T(8,128)(2,1)S(1)}, bf16[384,512]{1,0:T(8,128)(2,1)S(1)}, u32[]{:S(2)}, u32[]{:S(2)}) collective-permute-start(bf16[384,512]{1,0:T(8,128)(2,1)S(1)} %reshape.108.own), channel_id=1, source_target_pairs={{0,1},{1,2},{2,3},{3,0},{4,5},{5,6},{6,7},{7,4},{8,9},{9,10},{10,1... | collective-permute-start | bytes 1179656 | tf_op jit(solution)/shard_map/ppermute | solution.py:27
  109.8 24.8 %copy-start.1 = (f32[2048]{0:T(1024)S(1)}, f32[2048]{0:T(1024)}, u32[]{:S(2)}) copy-start(f32[2048]{0:T(1024)} %param.21) | copy-start | bytes 24580
  109.8 19.2 %collective-permute-start.20 = (bf16[512,512]{1,0:T(8,128)(2,1)S(1)}, bf16[512,512]{1,0:T(8,128)(2,1)S(1)}, u32[]{:S(2)}, u32[]{:S(2)}) collective-permute-start(bf16[512,512]{1,0:T(8,128)(2,1)S(1)} %slice_bitcast_fusion.own), channel_id=1, source_target_pairs={{0,3},{1,0},{2,1},{3,2},{4,7},{5,4},{6,5},{7,6},{8,11},{9,8},{10,9... | collective-permute-start | bytes 1572872 | tf_op jit(solution)/shard_map/ppermute | solution.py:27
  111.2 19.4 %collective-permute-start.19 = (bf16[512,512]{1,0:T(8,128)(2,1)S(1)}, bf16[512,512]{1,0:T(8,128)(2,1)S(1)}, u32[]{:S(2)}, u32[]{:S(2)}) collective-permute-start(bf16[512,512]{1,0:T(8,128)(2,1)S(1)} %slice_bitcast_fusion.own), channel_id=1, source_target_pairs={{0,1},{1,2},{2,3},{3,0},{4,5},{5,6},{6,7},{7,4},{8,9},{9,10},{10,1... | collective-permute-start | bytes 1572872 | tf_op jit(solution)/shard_map/ppermute | solution.py:27
  117.8 15.4 %collective-permute-start.14 = (bf16[192,512]{1,0:T(8,128)(2,1)S(1)}, bf16[192,512]{1,0:T(8,128)(2,1)S(1)}, u32[]{:S(2)}, u32[]{:S(2)}) collective-permute-start(bf16[192,512]{1,0:T(8,128)(2,1)S(1)} %slice.72), channel_id=1, source_target_pairs={{0,3},{1,0},{2,1},{3,2},{4,7},{5,4},{6,5},{7,6},{8,11},{9,8},{10,9... | collective-permute-start | bytes 589832 | tf_op jit(solution)/shard_map/ppermute | solution.py:27
  119.4 15.2 %collective-permute-start.13 = (bf16[192,512]{1,0:T(8,128)(2,1)S(1)}, bf16[192,512]{1,0:T(8,128)(2,1)S(1)}, u32[]{:S(2)}, u32[]{:S(2)}) collective-permute-start(bf16[192,512]{1,0:T(8,128)(2,1)S(1)} %slice.71), channel_id=1, source_target_pairs={{0,1},{1,2},{2,3},{3,0},{4,5},{5,6},{6,7},{7,4},{8,9},{9,10},{10,1... | collective-permute-start | bytes 589832 | tf_op jit(solution)/shard_map/ppermute | solution.py:27
  129.1 16.9 %collective-permute-start.22 = (bf16[256,512]{1,0:T(8,128)(2,1)S(1)}, bf16[256,512]{1,0:T(8,128)(2,1)S(1)}, u32[]{:S(2)}, u32[]{:S(2)}) collective-permute-start(bf16[256,512]{1,0:T(8,128)(2,1)S(1)} %slice.75), channel_id=1, source_target_pairs={{0,3},{1,0},{2,1},{3,2},{4,7},{5,4},{6,5},{7,6},{8,11},{9,8},{10,9... | collective-permute-start | bytes 786440 | tf_op jit(solution)/shard_map/ppermute | solution.py:27
  130.6 15.4 %collective-permute-start.21 = (bf16[256,512]{1,0:T(8,128)(2,1)S(1)}, bf16[256,512]{1,0:T(8,128)(2,1)S(1)}, u32[]{:S(2)}, u32[]{:S(2)}) collective-permute-start(bf16[256,512]{1,0:T(8,128)(2,1)S(1)} %slice.74), channel_id=1, source_target_pairs={{0,1},{1,2},{2,3},{3,0},{4,5},{5,6},{6,7},{7,4},{8,9},{9,10},{10,1... | collective-permute-start | bytes 786440 | tf_op jit(solution)/shard_map/ppermute | solution.py:27
  143.2 16.1 %collective-permute-start.15 = (bf16[192,512]{1,0:T(8,128)(2,1)S(1)}, bf16[192,512]{1,0:T(8,128)(2,1)S(1)}, u32[]{:S(2)}, u32[]{:S(2)}) collective-permute-start(bf16[192,512]{1,0:T(8,128)(2,1)S(1)} %get-tuple-element.27), channel_id=1, source_target_pairs={{0,1},{1,2},{2,3},{3,0},{4,5},{5,6},{6,7},{7,4},{8,9},{9,10},{10,1... | collective-permute-start | bytes 589832 | tf_op jit(solution)/shard_map/ppermute | solution.py:27
  143.3 15.9 %collective-permute-start.17 = (bf16[192,512]{1,0:T(8,128)(2,1)S(1)}, bf16[192,512]{1,0:T(8,128)(2,1)S(1)}, u32[]{:S(2)}, u32[]{:S(2)}) collective-permute-start(bf16[192,512]{1,0:T(8,128)(2,1)S(1)} %get-tuple-element.29), channel_id=1, source_target_pairs={{0,3},{1,0},{2,1},{3,2},{4,7},{5,4},{6,5},{7,6},{8,11},{9,8},{10,9... | collective-permute-start | bytes 589832 | tf_op jit(solution)/shard_map/ppermute | solution.py:27
  156.4 9.4 %collective-permute-start.23 = (bf16[256,512]{1,0:T(8,128)(2,1)S(1)}, bf16[256,512]{1,0:T(8,128)(2,1)S(1)}, u32[]{:S(2)}, u32[]{:S(2)}) collective-permute-start(bf16[256,512]{1,0:T(8,128)(2,1)S(1)} %get-tuple-element.32), channel_id=1, source_target_pairs={{0,1},{1,2},{2,3},{3,0},{4,5},{5,6},{6,7},{7,4},{8,9},{9,10},{10,1... | collective-permute-start | bytes 786440 | tf_op jit(solution)/shard_map/ppermute | solution.py:27
  156.5 6.0 %collective-permute-start.25 = (bf16[256,512]{1,0:T(8,128)(2,1)S(1)}, bf16[256,512]{1,0:T(8,128)(2,1)S(1)}, u32[]{:S(2)}, u32[]{:S(2)}) collective-permute-start(bf16[256,512]{1,0:T(8,128)(2,1)S(1)} %get-tuple-element.34), channel_id=1, source_target_pairs={{0,3},{1,0},{2,1},{3,2},{4,7},{5,4},{6,5},{7,6},{8,11},{9,8},{10,9... | collective-permute-start | bytes 786440 | tf_op jit(solution)/shard_map/ppermute | solution.py:27
  159.3 9.6 %collective-permute-start.18 = (bf16[384,512]{1,0:T(8,128)(2,1)S(1)}, bf16[384,512]{1,0:T(8,128)(2,1)S(1)}, u32[]{:S(2)}, u32[]{:S(2)}) collective-permute-start(bf16[384,512]{1,0:T(8,128)(2,1)S(1)} %fusion.35), channel_id=1, source_target_pairs={{0,3},{1,0},{2,1},{3,2},{4,7},{5,4},{6,5},{7,6},{8,11},{9,8},{10,9... | collective-permute-start | bytes 1179656 | tf_op jit(solution)/shard_map/ppermute | solution.py:27
  159.4 10.8 %collective-permute-start.16 = (bf16[384,512]{1,0:T(8,128)(2,1)S(1)}, bf16[384,512]{1,0:T(8,128)(2,1)S(1)}, u32[]{:S(2)}, u32[]{:S(2)}) collective-permute-start(bf16[384,512]{1,0:T(8,128)(2,1)S(1)} %fusion.34), channel_id=1, source_target_pairs={{0,1},{1,2},{2,3},{3,0},{4,5},{5,6},{6,7},{7,4},{8,9},{9,10},{10,1... | collective-permute-start | bytes 1179656 | tf_op jit(solution)/shard_map/ppermute | solution.py:27
  162.6 22.9 %collective-permute-start.26 = (bf16[512,512]{1,0:T(8,128)(2,1)S(1)}, bf16[512,512]{1,0:T(8,128)(2,1)S(1)}, u32[]{:S(2)}, u32[]{:S(2)}) collective-permute-start(bf16[512,512]{1,0:T(8,128)(2,1)S(1)} %fusion.30), channel_id=1, source_target_pairs={{0,3},{1,0},{2,1},{3,2},{4,7},{5,4},{6,5},{7,6},{8,11},{9,8},{10,9... | collective-permute-start | bytes 1572872 | tf_op jit(solution)/shard_map/ppermute | solution.py:27
  165.9 19.6 %collective-permute-start.24 = (bf16[512,512]{1,0:T(8,128)(2,1)S(1)}, bf16[512,512]{1,0:T(8,128)(2,1)}, u32[]{:S(2)}, u32[]{:S(2)}) collective-permute-start(bf16[512,512]{1,0:T(8,128)(2,1)S(1)} %fusion.29), channel_id=1, source_target_pairs={{0,1},{1,2},{2,3},{3,0},{4,5},{5,6},{6,7},{7,4},{8,9},{9,10},{10,1... | collective-permute-start | bytes 1572872 | tf_op jit(solution)/shard_map/ppermute | solution.py:27
  171.4 31.8 %all-to-all-start.1 = ((bf16[64,6,512]{2,1,0:T(8,128)(2,1)}), bf16[64,6,512]{2,1,0:T(8,128)(2,1)S(1)}, u32[]{:S(2)}, u32[]{:S(2)}) async-start(bf16[64,6,512]{2,1,0:T(8,128)(2,1)} %reshape.110), calls=%async_computation.1 | async-start | bytes 1048576 | tf_op jit(solution)/shard_map/all_to_all | solution.py:340
  185.5 23.4 %copy-start.10 = (f32[320,2]{0,1:T(2,128)S(1)}, f32[320,2]{0,1:T(2,128)}, u32[]{:S(2)}) copy-start(f32[320,2]{0,1:T(2,128)} %param.23) | copy-start | bytes 7684
  187.5 21.5 %copy-start.7 = (s32[320]{0:T(512)S(1)}, s32[320]{0:T(512)}, u32[]{:S(2)}) copy-start(s32[320]{0:T(512)} %get-tuple-element.38) | copy-start | bytes 3844
  203.2 23.4 %all-to-all-start.2 = ((bf16[64,8,512]{2,1,0:T(8,128)(2,1)}), bf16[64,8,512]{2,1,0:T(8,128)(2,1)S(1)}, u32[]{:S(2)}, u32[]{:S(2)}) async-start(bf16[64,8,512]{2,1,0:T(8,128)(2,1)} %fusion.22), calls=%async_computation.2 | async-start | bytes 1048576 | tf_op jit(solution)/shard_map/all_to_all | solution.py:340
  (9 other events, 91.4 us)
where the time goes:
time: 229 us; the launch traced here: 228 us
  waiting for transfers between devices  71.6 us (31%)
  starting transfers between devices  58.2 us (25%)
  blocking collectives  46.9 us (20%)
  Pallas kernels  34.2 us (15%)
  other arithmetic  7.4 us (3%)
  matrix products  7.2 us (3%)
    all_to_all x1, blocking collectives, layer(): block = lax.all_to_all(send, 'sp', 0, 0, tiled=True)  46.9 us
    all_to_all x2, waiting for transfers between devices, layer(): lax.all_to_all(result, 'sp', 0, 0, tiled=True)  32.2 us
    ppermute x23, waiting for transfers between devices, rotated(): return lax.ppermute(x, axis, [(i, (i + by) % size) for i in range(size)])  30.4 us
    ppermute x23, starting transfers between devices, rotated(): return lax.ppermute(x, axis, [(i, (i + by) % size) for i in range(size)])  27.6 us
    all_to_all x2, starting transfers between devices, layer(): lax.all_to_all(result, 'sp', 0, 0, tiled=True)  19.8 us
    pallas_call x2, Pallas kernels, experts_of(): pl.pallas_call(expert_body, out_shape=[shape(rows // 2), shape(rows // 2)...  19.1 us
    pallas_call x3, Pallas kernels, attend(): pl.pallas_call(functools.partial(attend_body, own, last, heads), out_shap...  15.1 us
    ppermute x2, waiting for transfers between devices, shifted(): lax.ppermute(x, axis, [(i, i + by) for i in range(size) if 0 <= i + by <...  8.98 us
  transfers between devices with their start and end apart: 29, of which 13 were waited for; matrix products, arithmetic and copies ran while one was open for 4% of the time, Pallas kernels for 15%

commit v1 on v0

--- a/solution.py
+++ b/solution.py
@@ -29,10 +29,10 @@
 
 def attend_body(own, last, heads, *refs):
     if last:
-        *refs, shift_scr, blk_scr, acc_ref, tot_ref = refs
+        *refs, bias_scr, shift_scr, blk_scr, acc_ref, tot_ref = refs
         refs = (*refs, acc_ref, tot_ref)
     else:
-        *refs, shift_scr, blk_scr = refs
+        *refs, bias_scr, shift_scr, blk_scr = refs
     if own:
         q_ref, blk_ref, tri_ref, qdoc_ref, acc_ref, tot_ref = refs
     elif last:
@@ -46,7 +46,7 @@
     groups = [(lo, min(keys, lo + 128)) for lo in range(0, keys, 128)]
     lane = lax.broadcasted_iota(jnp.int32, (rows, 128), 1)
 
-    def one_head(blk, admitted, acc_old, tot_old, head):
+    def one_head(blk, acc_old, tot_old, head):
         pair = head // 2
         cols = pl.ds(pl.multiple_of(128 * pair, 128), 128)
         v_cols = pl.ds(pl.multiple_of(width + 128 * pair, 128), 128)
@@ -57,23 +57,22 @@
         shift = shift_scr[pl.ds(head, 1), :]
         scores = lax.dot_general(q_head, blk[0:keys, cols], (((1,), (1,)), ((), ())), preferred_element_type=F32)
         sticks = []
-        for (lo, hi), ok in reversed(list(zip(groups, admitted))):
+        for lo, hi in reversed(groups):
             size = hi - lo
-            s = scores[:, lo:hi] * (LOG2E * HEAD ** (-0.5)) + shift[:, lo:hi]
+            s = scores[:, lo:hi] * (LOG2E * HEAD ** (-0.5)) + shift[:, lo:hi] + bias_scr[:, lo:hi]
             drop = jnp.maximum(s, 0.0) + jnp.log2(1.0 + jnp.exp2(-jnp.abs(s)))
-            rest = jnp.where(ok, drop, 0.0)
-            high = rest.astype(BF16)
-            low = (rest - high.astype(F32)).astype(BF16)
+            high = drop.astype(BF16)
+            low = (drop - high.astype(F32)).astype(BF16)
             if size == 128:
                 sums = jnp.dot(jnp.concatenate([high, low], axis=1), tri_ref[...], preferred_element_type=F32)
             else:
                 sums = jnp.dot(high, tri_ref[0:size], preferred_element_type=F32) + jnp.dot(
                     low, tri_ref[0:size], preferred_element_type=F32
                 )
-            z = (s - drop) + sums[:, 0:size]
+            z = s + sums[:, 0:size]
             if later is not None:
                 z = z + later[:, 0:size]
-            sticks.append(jnp.where(ok, jnp.exp2(z), 0.0).astype(BF16))
+            sticks.append(jnp.exp2(z).astype(BF16))
             gone = sums[:, 128:256]
             later = gone if later is None else later + gone
         stick = jnp.concatenate(sticks[::-1], axis=1)
@@ -85,15 +84,13 @@
     def one_block(blk, acc_old, tot_old):
         extra = blk[keys : keys + EXTRA, 0:keys].astype(F32)
         shift_scr[...] = extra * LOG2E
-        admitted = []
-        for lo, hi in groups:
-            ok = extra[heads : heads + 1, lo:hi] == qdoc_ref[...]
-            if own:
-                q_iota = lax.broadcasted_iota(jnp.int32, (rows, hi - lo), 0)
-                k_iota = lax.broadcasted_iota(jnp.int32, (rows, hi - lo), 1) + lo
-                ok = ok & (k_iota < q_iota)
-            admitted.append(ok)
-        lax.fori_loop(0, heads, lambda h, _: (one_head(blk, admitted, acc_old, tot_old, h), 0)[1], 0)
+        ok = extra[heads : heads + 1, :] == qdoc_ref[...]
+        if own:
+            q_iota = lax.broadcasted_iota(jnp.int32, (rows, keys), 0)
+            k_iota = lax.broadcasted_iota(jnp.int32, (rows, keys), 1)
+            ok = ok & (k_iota < q_iota)
+        bias_scr[...] = jnp.where(ok, 0.0, -1e30)
+        lax.fori_loop(0, heads, lambda h, _: (one_head(blk, acc_old, tot_old, h), 0)[1], 0)
 
     if own:
         acc_ref[...] = jnp.zeros_like(acc_ref)
@@ -102,14 +99,16 @@
         acc_ref[...] = acc_in[...]
         tot_ref[...] = tot_in[...]
 
+        def copy_rows(ref, r):
+            here = pl.ds(pl.multiple_of(48 * r, 48), 48)
+            blk_scr[here] = ref[here]
+
         def visit(t, _):
-            @pl.when(t == 0)
-            def _():
-                blk_scr[...] = near_ref[...]
-
-            @pl.when(t == 1)
-            def _():
-                blk_scr[...] = far_ref[...]
+            for n, ref in enumerate((near_ref, far_ref)):
+
+                @pl.when(t == n)
+                def _(ref=ref):
+                    lax.fori_loop(0, ref.shape[0] // 48, lambda r, _: (copy_rows(ref, r), 0)[1], 0)
 
             one_block(blk_scr, acc_ref, tot_ref)
             return 0
@@ -133,7 +132,7 @@
     return pl.pallas_call(
         functools.partial(attend_body, own, last, heads),
         out_shape=outs,
-        scratch_shapes=[pltpu.VMEM((EXTRA, keys), F32), pltpu.VMEM(blks[0].shape, BF16)] + scratch,
+        scratch_shapes=[pltpu.VMEM((rows, keys), F32), pltpu.VMEM((EXTRA, keys), F32), pltpu.VMEM(blks[0].shape, BF16)] + scratch,
         name="attend_own" if own else "attend_visit",
         cost_estimate=pl.CostEstimate(
             flops=len(blks) * 2 * heads * rows * keys * (2 * HEAD + 2 * keys),
@@ -194,11 +193,19 @@
         return 0
 
     lax.fori_loop(0, 4, down, 0)
-    out_ft[...] = norm[0, :half]
-    out_fb[...] = norm[0, half:]
-    out_up[...] = norm[1]
-    out_down[...] = norm[2]
-    out_own[...] = norm[3]
+
+    def spread(t, _):
+        top = pl.ds(pl.multiple_of(32 * t, 32), 32)
+        low = pl.ds(pl.multiple_of(half + 32 * t, 32), 32)
+        out_ft[top] = norm[0, top]
+        out_fb[top] = norm[0, low]
+        for rows in (top, low):
+            out_up[rows] = norm[1, rows]
+            out_down[rows] = norm[2, rows]
+            out_own[rows] = norm[3, rows]
+        return 0
+
+    lax.fori_loop(0, half // 32, spread, 0)
 
 
 def experts_of(take, own, left, right, opp_t, opp_b, gain, gate_w, up_w, down_w):
@@ -284,7 +291,7 @@
     size = lax.axis_size("sp")
     swap = lambda x: lax.ppermute(x, "sp", [(i, i ^ 1) for i in range(size)])
     two = shifted(packed, "sp", 2)
-    four = shifted(two, "sp", 2)
+    four = shifted(packed, "sp", 4)
     one = swap(jnp.where(odd, two, packed))
     held = lax.optimization_barrier((two, one))[0]
     three = swap(jnp.where(odd, four, held))
@@ -299,7 +306,7 @@
     iota = jnp.arange(rows, dtype=jnp.int32)
     later = (iota[:, None] > iota[None, :]).astype(BF16)
     lanes = jnp.arange(128, dtype=jnp.int32)
-    tri = jnp.where(lanes[:, None] > lanes[None, :], -1.0, 0.0)
+    tri = jnp.where(lanes[:, None] >= lanes[None, :], -1.0, 0.0)
     tri = jnp.concatenate([tri, jnp.full((128, 128), -1.0)], axis=1).astype(BF16)
     tri = jnp.concatenate([tri, tri], axis=0)
     state = attend(True, False, heads, query_rows, (packed,), tri, qdoc, ())
@@ -316,8 +323,8 @@
     earlier = jnp.dot(later, count, preferred_element_type=F32)
     ids = [expert_ids[:, k : k + 1] for k in range(top)]
     slot = [jnp.sum(jnp.where(c, earlier, 0.0), axis=1, keepdims=True).astype(jnp.int32) for c in chosen]
-    targets = jnp.arange(experts * capacity, dtype=jnp.int32)[None]
-    select = sum((i * capacity + s == targets).astype(BF16) for i, s in zip(ids, slot))
+    targets = jnp.arange(experts * capacity, dtype=jnp.int32)[:, None]
+    select = sum((jnp.transpose(i * capacity + s) == targets).astype(BF16) for i, s in zip(ids, slot))
 
     left, right, opp_t, opp_b = gather_tp(attended)
     opp = jnp.concatenate([opp_t, opp_b], axis=0)
@@ -325,18 +332,20 @@
     projected = part(attended, w_own) + part(left, w_left) + part(right, w_right) + part(opp, w_opp)
     middle = (stream.astype(F32) + projected).astype(BF16)
 
-    send = lax.dot_general(select, middle, (((0,), (0,)), ((), ())), preferred_element_type=F32)
-    send = send.astype(BF16).reshape(experts, capacity, cols)
+    tiles = cols // 128
+    send = jnp.dot(select, middle, preferred_element_type=F32)
+    send = send.astype(BF16).reshape(experts, capacity * tiles, 128)
     block = lax.all_to_all(send, "sp", 0, 0, tiled=True)
     take = lax.rem(jnp.array([0, 3, 1, 2, 2, 1, 3, 0], jnp.int32) + me, 4)
     gain = norm_gain.reshape(4, 1, cols)
     mixed = middle.astype(F32)
-    for lo, hi in ((8, capacity), (0, 8)):
+    for lo, hi in ((0, 8), (8, capacity)):
         items = hi - lo
-        part = block[:, lo:hi].reshape(experts * items, cols)
+        shape = (experts, items, cols) if items % 8 == 0 else (experts, items * tiles, 128)
+        part = block[:, lo * tiles : hi * tiles].reshape(experts * items, cols)
         wide = gather_tp(part)
         parts = experts_of(take, part, *wide, gain, gate_weight, up_weight, down_weight)
-        result = scatter_sum_tp(parts, (experts, items, cols))
+        result = scatter_sum_tp(parts, shape)
         back = lax.all_to_all(result, "sp", 0, 0, tiled=True).reshape(experts * items, cols)
 
         slots = jnp.arange(experts * items, dtype=jnp.int32)[None]

time: 229 us -> 223 us (0.974)
  blocking collectives: 46.9 us -> 42.9 us
    all_to_all x1, blocking collectives: 46.9 us -> 42.9 us  [layer(): block = lax.all_to_all(send, 'sp', 0, 0, tiled=True)]
    all_to_all x2, waiting for transfers between devices: 32.2 us -> 29.7 us  [layer(): lax.all_to_all(result, 'sp', 0, 0, tiled=True)]
where the time goes in v1:
time: 223 us
  waiting for transfers between devices  69.4 us (31%)
  starting transfers between devices  58.7 us (26%)
  blocking collectives  42.9 us (19%)
  Pallas kernels  33.9 us (15%)
  other arithmetic  7.4 us (3%)
  matrix products  7.03 us (3%)
  local copies, waits for them, and re-layouts  2.87 us (1%)
    all_to_all x1, blocking collectives, layer(): block = lax.all_to_all(send, 'sp', 0, 0, tiled=True)  42.9 us
    ppermute x23, waiting for transfers between devices, rotated(): return lax.ppermute(x, axis, [(i, (i + by) % size) for i in range(size)])  30.8 us
    all_to_all x2, waiting for transfers between devices, layer(): lax.all_to_all(result, 'sp', 0, 0, tiled=True)  29.7 us
    ppermute x23, starting transfers between devices, rotated(): return lax.ppermute(x, axis, [(i, (i + by) % size) for i in range(size)])  27.7 us
    pallas_call x2, Pallas kernels, experts_of(): pl.pallas_call(expert_body, out_shape=[shape(rows // 2), shape(rows // 2)...  19.1 us
    all_to_all x2, starting transfers between devices, layer(): lax.all_to_all(result, 'sp', 0, 0, tiled=True)  18.7 us
    pallas_call x3, Pallas kernels, attend(): pl.pallas_call(functools.partial(attend_body, own, last, heads), out_shap...  14.8 us
    ppermute x2, starting transfers between devices, shifted(): lax.ppermute(x, axis, [(i, i + by) for i in range(size) if 0 <= i + by <...  9.77 us
  transfers between devices with their start and end apart: 29, of which 13 were waited for; matrix products, arithmetic and copies ran while one was open for 4% of the time, Pallas kernels for 15%

profile of v1, /device:TPU:1, one launch (start us, length us, event | category | flops | bytes accessed | tf_op | source)
XLA Modules:
  0.0 222.9 jit_solution(13202153290326984753)
XLA Ops:
  3.2 4.0 %collective-permute-start.1 = (bf16[336,512]{1,0:T(8,128)(2,1)S(1)}, bf16[336,512]{1,0:T(8,128)(2,1)S(1)}, u32[]{:S(2)}, u32[]{:S(2)}) collective-permute-start(bf16[336,512]{1,0:T(8,128)(2,1)S(1)} %fusion.26.refs_1_), channel_id=1, source_target_pairs={{0,8},{4,12},{8,16},{12,20},{16,24},{20,28},{24,32},{28,36},{32,40... | collective-permute-start | bytes 1032200 | tf_op jit(solution)/shard_map/ppermute | solution.py:22
  7.3 6.7 %collective-permute-done.1.refs_2_ = bf16[336,512]{1,0:T(8,128)(2,1)S(1)} collective-permute-done((bf16[336,512]{1,0:T(8,128)(2,1)S(1)}, bf16[336,512]{1,0:T(8,128)(2,1)S(1)}, u32[]{:S(2)}, u32[]{:S(2)}) %collective-permute-start.1) | collective-permute-done | bytes 344096 | tf_op jit(solution)/shard_map/ppermute | solution.py:22
  15.1 1.6 collective-permute-start.2
  16.7 5.7 %collective-permute-start = (bf16[336,512]{1,0:T(8,128)(2,1)S(1)}, bf16[336,512]{1,0:T(8,128)(2,1)S(1)}, u32[]{:S(2)}, u32[]{:S(2)}) collective-permute-start(bf16[336,512]{1,0:T(8,128)(2,1)S(1)} %fusion.26.refs_1_), channel_id=1, source_target_pairs={{0,16},{4,20},{8,24},{12,28},{16,32},{20,36},{24,40},{28,44},{32,4... | collective-permute-start | bytes 1032200 | tf_op jit(solution)/shard_map/ppermute | solution.py:22
  23.8 2.5 %collective-permute-start.10 = (bf16[256,512]{1,0:T(8,128)(2,1)S(1)}, bf16[256,512]{1,0:T(8,128)(2,1)}, u32[]{:S(2)}, u32[]{:S(2)}) collective-permute-start(bf16[256,512]{1,0:T(8,128)(2,1)S(1)} %get-tuple-element.51), channel_id=1, source_target_pairs={{0,2},{1,3},{2,0},{3,1},{4,6},{5,7},{6,4},{7,5},{8,10},{9,11},{10,... | collective-permute-start | bytes 786440 | tf_op jit(solution)/shard_map/ppermute | solution.py:27
  27.5 2.3 %collective-permute-done.refs_2_ = bf16[336,512]{1,0:T(8,128)(2,1)S(1)} collective-permute-done((bf16[336,512]{1,0:T(8,128)(2,1)S(1)}, bf16[336,512]{1,0:T(8,128)(2,1)S(1)}, u32[]{:S(2)}, u32[]{:S(2)}) %collective-permute-start) | collective-permute-done | bytes 344096 | tf_op jit(solution)/shard_map/ppermute | solution.py:22
  30.9 2.9 %attend_own.1 = (f32[320,256]{1,0:T(8,128)S(1)}, f32[320,512]{1,0:T(8,128)S(1)}) custom-call(bf16[320,256]{1,0:T(8,128)(2,1)S(1)} %copy-done, bf16[336,512]{1,0:T(8,128)(2,1)S(1)} %fusion.26.refs_1_, bf16[256,256]{1,0:T(8,128)(2,1)S(1)} %pad_maximum_fusion.refs_2_.refs_3_, f32[320,1]{1,0:T(8,128)S(1)} %broadcast_in_dim.44.refs_3_.refs_4_), custom_call_target="tpu_custom_call" | custom-call | flops 629145600 | bytes 671744 | tf_op jit(solution)/shard_map/attend_own/pallas_call | solution.py:132
  33.8 6.0 %attend_visit.2 = (f32[320,256]{1,0:T(8,128)S(1)}, f32[320,512]{1,0:T(8,128)S(1)}) custom-call(bf16[320,256]{1,0:T(8,128)(2,1)S(1)} %copy-done, bf16[336,512]{1,0:T(8,128)(2,1)S(1)} %collective-permute-done.2.refs_1_, bf16[336,512]{1,0:T(8,128)(2,1)S(1)} %collective-permute-done.1.refs_2_, bf16[256,256]{1,0:T(8,128)(2,1)S(1)} %pad_maximum_fusion.refs_2_.refs_3_, ...), custom_call_target="tpu_custom_call" | custom-call | flops 1258291200 | bytes 1015808 | tf_op jit(solution)/shard_map/attend_visit/pallas_call | solution.py:132
  39.8 6.0 %attend_visit.3 = bf16[320,256]{1,0:T(8,128)(2,1)S(1)} custom-call(bf16[320,256]{1,0:T(8,128)(2,1)S(1)} %copy-done, bf16[336,512]{1,0:T(8,128)(2,1)S(1)} %collective-permute-done.3.refs_1_, bf16[336,512]{1,0:T(8,128)(2,1)S(1)} %collective-permute-done.refs_2_, bf16[256,256]{1,0:T(8,128)(2,1)S(1)} %pad_maximum_fusion.refs_2_.refs_3_, ...), custom_call_target="tpu_custom_call" | custom-call | flops 1258291200 | bytes 1015808 | tf_op jit(solution)/shard_map/attend_visit/pallas_call | solution.py:132
  45.8 2.6 %collective-permute-start.6 = (bf16[320,256]{1,0:T(8,128)(2,1)S(1)}, bf16[320,256]{1,0:T(8,128)(2,1)S(1)}, u32[]{:S(2)}, u32[]{:S(2)}) collective-permute-start(bf16[320,256]{1,0:T(8,128)(2,1)S(1)} %attend_visit.3), channel_id=1, source_target_pairs={{0,3},{1,0},{2,1},{3,2},{4,7},{5,4},{6,5},{7,6},{8,11},{9,8},{10,9... | collective-permute-start | bytes 491528 | tf_op jit(solution)/shard_map/ppermute | solution.py:27
  49.2 2.6 %collective-permute-done.6 = bf16[320,256]{1,0:T(8,128)(2,1)S(1)} collective-permute-done((bf16[320,256]{1,0:T(8,128)(2,1)S(1)}, bf16[320,256]{1,0:T(8,128)(2,1)S(1)}, u32[]{:S(2)}, u32[]{:S(2)}) %collective-permute-start.6) | collective-permute-done | bytes 163872 | tf_op jit(solution)/shard_map/ppermute | solution.py:27
  51.9 3.4 %collective-permute-start.9 = (bf16[160,256]{1,0:T(8,128)(2,1)S(1)}, bf16[160,256]{1,0:T(8,128)(2,1)S(1)}, u32[]{:S(2)}, u32[]{:S(2)}) collective-permute-start(bf16[160,256]{1,0:T(8,128)(2,1)S(1)} %slice.69), channel_id=1, source_target_pairs={{0,3},{1,0},{2,1},{3,2},{4,7},{5,4},{6,5},{7,6},{8,11},{9,8},{10,9... | collective-permute-start | bytes 245768 | tf_op jit(solution)/shard_map/ppermute | solution.py:27
  57.8 2.1 collective-permute-done.8
  62.6 42.9 %all_to_all.15 = bf16[64,56,128]{2,1,0:T(8,128)(2,1)S(1)} all-to-all(bf16[64,56,128]{2,1,0:T(8,128)(2,1)S(1)} %reshape.109), channel_id=1, replica_groups=mesh['sp'=64,'tp'=4] {'sp'}, dimensions={0} | all-to-all | bytes 1835008 | tf_op jit(solution)/shard_map/all_to_all | solution.py:338
  109.3 6.4 %collective-permute-done.20.right = bf16[384,512]{1,0:T(8,128)(2,1)S(1)} collective-permute-done((bf16[384,512]{1,0:T(8,128)(2,1)S(1)}, bf16[384,512]{1,0:T(8,128)(2,1)S(1)}, u32[]{:S(2)}, u32[]{:S(2)}) %collective-permute-start.20) | collective-permute-done | bytes 393248 | tf_op jit(solution)/shard_map/ppermute | solution.py:27
  115.7 1.6 collective-permute-start.22
  117.4 9.5 %collective-permute-done.12.right = bf16[512,512]{1,0:T(8,128)(2,1)S(1)} collective-permute-done((bf16[512,512]{1,0:T(8,128)(2,1)S(1)}, bf16[512,512]{1,0:T(8,128)(2,1)S(1)}, u32[]{:S(2)}, u32[]{:S(2)}) %collective-permute-start.12) | collective-permute-done | bytes 524320 | tf_op jit(solution)/shard_map/ppermute | solution.py:27
  126.9 1.6 collective-permute-start.14
  128.6 2.5 %collective-permute-done.22.opp_b = bf16[192,512]{1,0:T(8,128)(2,1)S(1)} collective-permute-done((bf16[192,512]{1,0:T(8,128)(2,1)S(1)}, bf16[192,512]{1,0:T(8,128)(2,1)S(1)}, u32[]{:S(2)}, u32[]{:S(2)}) %collective-permute-start.22) | collective-permute-done | bytes 196640 | tf_op jit(solution)/shard_map/ppermute | solution.py:27
  132.4 8.7 %experts.3 = (bf16[192,512]{1,0:T(8,128)(2,1)S(1)}, bf16[192,512]{1,0:T(8,128)(2,1)S(1)}, bf16[384,512]{1,0:T(8,128)(2,1)S(1)}, bf16[384,512]{1,0:T(8,128)(2,1)S(1)}, bf16[384,512]{1,0:T(8,128)(2,1)S(1)}) custom-call(s32[8]{0:T(128)S(1)} %compare_select_fusion.take_ref, bf16[384,512]{1,0:T(8,128)(2,1)S(1)} %reshape.114.own, ...), custom_call_target="tpu_custom_call" | custom-call | flops 4227858432 | bytes 14155776 | tf_op jit(solution)/shard_map/experts/pallas_call | solution.py:218
  141.2 2.7 %collective-permute-start.25 = (bf16[192,512]{1,0:T(8,128)(2,1)S(1)}, bf16[192,512]{1,0:T(8,128)(2,1)S(1)}, u32[]{:S(2)}, u32[]{:S(2)}) collective-permute-start(bf16[192,512]{1,0:T(8,128)(2,1)S(1)} %get-tuple-element.34), channel_id=1, source_target_pairs={{0,3},{1,0},{2,1},{3,2},{4,7},{5,4},{6,5},{7,6},{8,11},{9,8},{10,9... | collective-permute-start | bytes 589832 | tf_op jit(solution)/shard_map/ppermute | solution.py:27
  143.9 10.5 %experts.2 = (bf16[256,512]{1,0:T(8,128)(2,1)S(1)}, bf16[256,512]{1,0:T(8,128)(2,1)S(1)}, bf16[512,512]{1,0:T(8,128)(2,1)S(1)}, bf16[512,512]{1,0:T(8,128)(2,1)S(1)}, bf16[512,512]{1,0:T(8,128)(2,1)S(1)}) custom-call(s32[8]{0:T(128)S(1)} %compare_select_fusion.take_ref, bf16[512,512]{1,0:T(8,128)(2,1)S(1)} %reshape.110.own, ...), custom_call_target="tpu_custom_call" | custom-call | flops 5637144576 | bytes 15204352 | tf_op jit(solution)/shard_map/experts/pallas_call | solution.py:218
  154.4 2.7 %collective-permute-start.17 = (bf16[256,512]{1,0:T(8,128)(2,1)S(1)}, bf16[256,512]{1,0:T(8,128)(2,1)S(1)}, u32[]{:S(2)}, u32[]{:S(2)}) collective-permute-start(bf16[256,512]{1,0:T(8,128)(2,1)S(1)} %get-tuple-element.29), channel_id=1, source_target_pairs={{0,3},{1,0},{2,1},{3,2},{4,7},{5,4},{6,5},{7,6},{8,11},{9,8},{10,9... | collective-permute-start | bytes 786440 | tf_op jit(solution)/shard_map/ppermute | solution.py:27
  157.3 1.5 collective-permute-start.24
  158.8 1.6 collective-permute-done.17
  160.5 3.2 %collective-permute-start.18 = (bf16[512,512]{1,0:T(8,128)(2,1)S(1)}, bf16[512,512]{1,0:T(8,128)(2,1)S(1)}, u32[]{:S(2)}, u32[]{:S(2)}) collective-permute-start(bf16[512,512]{1,0:T(8,128)(2,1)S(1)} %fusion.30), channel_id=1, source_target_pairs={{0,3},{1,0},{2,1},{3,2},{4,7},{5,4},{6,5},{7,6},{8,11},{9,8},{10,9... | collective-permute-start | bytes 1572872 | tf_op jit(solution)/shard_map/ppermute | solution.py:27
  163.9 3.4 %collective-permute-done.26 = bf16[384,512]{1,0:T(8,128)(2,1)S(1)} collective-permute-done((bf16[384,512]{1,0:T(8,128)(2,1)S(1)}, bf16[384,512]{1,0:T(8,128)(2,1)S(1)}, u32[]{:S(2)}, u32[]{:S(2)}) %collective-permute-start.26) | collective-permute-done | bytes 393248 | tf_op jit(solution)/shard_map/ppermute | solution.py:27
  169.8 13.2 %all-to-all-start.2 = ((bf16[64,24,128]{2,1,0:T(8,128)(2,1)}), bf16[64,24,128]{2,1,0:T(8,128)(2,1)S(1)}, u32[]{:S(2)}, u32[]{:S(2)}) async-start(bf16[64,24,128]{2,1,0:T(8,128)(2,1)} %reshape.115), calls=%async_computation.2 | async-start | bytes 786432 | tf_op jit(solution)/shard_map/all_to_all | solution.py:349
  183.1 2.0 fusion.22
  185.1 13.1 %all-to-all-done.2 = bf16[64,24,128]{2,1,0:T(8,128)(2,1)S(1)} async-done(((bf16[64,24,128]{2,1,0:T(8,128)(2,1)}), bf16[64,24,128]{2,1,0:T(8,128)(2,1)S(1)}, u32[]{:S(2)}, u32[]{:S(2)}) %all-to-all-start.2) | async-done | bytes 393248 | tf_op jit(solution)/shard_map/all_to_all | solution.py:349
  198.2 5.4 %all-to-all-start.1 = ((bf16[64,8,512]{2,1,0:T(8,128)(2,1)}), bf16[64,8,512]{2,1,0:T(8,128)(2,1)S(1)}, u32[]{:S(2)}, u32[]{:S(2)}) async-start(bf16[64,8,512]{2,1,0:T(8,128)(2,1)} %fusion.22), calls=%async_computation.1 | async-start | bytes 1048576 | tf_op jit(solution)/shard_map/all_to_all | solution.py:349
  204.7 16.6 %all-to-all-done.1 = bf16[64,8,512]{2,1,0:T(8,128)(2,1)S(1)} async-done(((bf16[64,8,512]{2,1,0:T(8,128)(2,1)}), bf16[64,8,512]{2,1,0:T(8,128)(2,1)S(1)}, u32[]{:S(2)}, u32[]{:S(2)}) %all-to-all-start.1) | async-done | bytes 524320 | tf_op jit(solution)/shard_map/all_to_all | solution.py:349
  (104 shorter events, 25.1 us)
Async XLA Ops:
  0.0 22.4 %copy-start.2 = (bf16[256,2048]{1,0:T(8,128)(2,1)S(1)}, bf16[256,2048]{1,0:T(8,128)(2,1)}, u32[]{:S(2)}) copy-start(bf16[256,2048]{1,0:T(8,128)(2,1)} %param.19) | copy-start | bytes 3145732
  3.2 10.8 %collective-permute-start.1 = (bf16[336,512]{1,0:T(8,128)(2,1)S(1)}, bf16[336,512]{1,0:T(8,128)(2,1)S(1)}, u32[]{:S(2)}, u32[]{:S(2)}) collective-permute-start(bf16[336,512]{1,0:T(8,128)(2,1)S(1)} %fusion.26.refs_1_), channel_id=1, source_target_pairs={{0,8},{4,12},{8,16},{12,20},{16,24},{20,28},{24,32},{28,36},{32,40... | collective-permute-start | bytes 1032200 | tf_op jit(solution)/shard_map/ppermute | solution.py:22
  15.1 12.4 %collective-permute-start.2 = (bf16[336,512]{1,0:T(8,128)(2,1)S(1)}, bf16[336,512]{1,0:T(8,128)(2,1)S(1)}, u32[]{:S(2)}, u32[]{:S(2)}) collective-permute-start(bf16[336,512]{1,0:T(8,128)(2,1)S(1)} %broadcast_select_fusion.1), channel_id=1, source_target_pairs={{0,4},{4,0},{8,12},{12,8},{16,20},{20,16},{24,28},{28,24},{32,36},... | collective-permute-start | bytes 1032200 | tf_op jit(solution)/shard_map/ppermute | solution.py:292
  16.7 13.1 %collective-permute-start = (bf16[336,512]{1,0:T(8,128)(2,1)S(1)}, bf16[336,512]{1,0:T(8,128)(2,1)S(1)}, u32[]{:S(2)}, u32[]{:S(2)}) collective-permute-start(bf16[336,512]{1,0:T(8,128)(2,1)S(1)} %fusion.26.refs_1_), channel_id=1, source_target_pairs={{0,16},{4,20},{8,24},{12,28},{16,32},{20,36},{24,40},{28,44},{32,4... | collective-permute-start | bytes 1032200 | tf_op jit(solution)/shard_map/ppermute | solution.py:22
  22.6 32.9 %collective-permute-start.5 = (bf16[256,512]{1,0:T(8,128)(2,1)S(1)}, bf16[256,512]{1,0:T(8,128)(2,1)}, u32[]{:S(2)}, u32[]{:S(2)}) collective-permute-start(bf16[256,512]{1,0:T(8,128)(2,1)S(1)} %get-tuple-element.50), channel_id=1, source_target_pairs={{0,1},{1,2},{2,3},{3,0},{4,5},{5,6},{6,7},{7,4},{8,9},{9,10},{10,1... | collective-permute-start | bytes 786440 | tf_op jit(solution)/shard_map/ppermute | solution.py:27
  23.8 34.0 %collective-permute-start.10 = (bf16[256,512]{1,0:T(8,128)(2,1)S(1)}, bf16[256,512]{1,0:T(8,128)(2,1)}, u32[]{:S(2)}, u32[]{:S(2)}) collective-permute-start(bf16[256,512]{1,0:T(8,128)(2,1)S(1)} %get-tuple-element.51), channel_id=1, source_target_pairs={{0,2},{1,3},{2,0},{3,1},{4,6},{5,7},{6,4},{7,5},{8,10},{9,11},{10,... | collective-permute-start | bytes 786440 | tf_op jit(solution)/shard_map/ppermute | solution.py:27
  26.3 30.3 %collective-permute-start.7 = (bf16[256,512]{1,0:T(8,128)(2,1)S(1)}, bf16[256,512]{1,0:T(8,128)(2,1)}, u32[]{:S(2)}, u32[]{:S(2)}) collective-permute-start(bf16[256,512]{1,0:T(8,128)(2,1)S(1)} %get-tuple-element.52), channel_id=1, source_target_pairs={{0,3},{1,0},{2,1},{3,2},{4,7},{5,4},{6,5},{7,6},{8,11},{9,8},{10,9... | collective-permute-start | bytes 786440 | tf_op jit(solution)/shard_map/ppermute | solution.py:27
  29.8 10.0 %collective-permute-start.3 = (bf16[336,512]{1,0:T(8,128)(2,1)S(1)}, bf16[336,512]{1,0:T(8,128)(2,1)S(1)}, u32[]{:S(2)}, u32[]{:S(2)}) collective-permute-start(bf16[336,512]{1,0:T(8,128)(2,1)S(1)} %broadcast_select_fusion), channel_id=1, source_target_pairs={{0,4},{4,0},{8,12},{12,8},{16,20},{20,16},{24,28},{28,24},{32,36},... | collective-permute-start | bytes 1032200 | tf_op jit(solution)/shard_map/ppermute | solution.py:292
  45.8 6.1 %collective-permute-start.6 = (bf16[320,256]{1,0:T(8,128)(2,1)S(1)}, bf16[320,256]{1,0:T(8,128)(2,1)S(1)}, u32[]{:S(2)}, u32[]{:S(2)}) collective-permute-start(bf16[320,256]{1,0:T(8,128)(2,1)S(1)} %attend_visit.3), channel_id=1, source_target_pairs={{0,3},{1,0},{2,1},{3,2},{4,7},{5,4},{6,5},{7,6},{8,11},{9,8},{10,9... | collective-permute-start | bytes 491528 | tf_op jit(solution)/shard_map/ppermute | solution.py:27
  48.3 7.0 %collective-permute-start.4 = (bf16[320,256]{1,0:T(8,128)(2,1)S(1)}, bf16[320,256]{1,0:T(8,128)(2,1)S(1)}, u32[]{:S(2)}, u32[]{:S(2)}) collective-permute-start(bf16[320,256]{1,0:T(8,128)(2,1)S(1)} %attend_visit.3), channel_id=1, source_target_pairs={{0,1},{1,2},{2,3},{3,0},{4,5},{5,6},{6,7},{7,4},{8,9},{9,10},{10,1... | collective-permute-start | bytes 491528 | tf_op jit(solution)/shard_map/ppermute | solution.py:27
  51.9 5.9 %collective-permute-start.9 = (bf16[160,256]{1,0:T(8,128)(2,1)S(1)}, bf16[160,256]{1,0:T(8,128)(2,1)S(1)}, u32[]{:S(2)}, u32[]{:S(2)}) collective-permute-start(bf16[160,256]{1,0:T(8,128)(2,1)S(1)} %slice.69), channel_id=1, source_target_pairs={{0,3},{1,0},{2,1},{3,2},{4,7},{5,4},{6,5},{7,6},{8,11},{9,8},{10,9... | collective-permute-start | bytes 245768 | tf_op jit(solution)/shard_map/ppermute | solution.py:27
  55.3 4.6 %collective-permute-start.8 = (bf16[160,256]{1,0:T(8,128)(2,1)S(1)}, bf16[160,256]{1,0:T(8,128)(2,1)S(1)}, u32[]{:S(2)}, u32[]{:S(2)}) collective-permute-start(bf16[160,256]{1,0:T(8,128)(2,1)S(1)} %slice.68), channel_id=1, source_target_pairs={{0,1},{1,2},{2,3},{3,0},{4,5},{5,6},{6,7},{7,4},{8,9},{9,10},{10,1... | collective-permute-start | bytes 245768 | tf_op jit(solution)/shard_map/ppermute | solution.py:27
  105.8 9.8 %collective-permute-start.20 = (bf16[384,512]{1,0:T(8,128)(2,1)S(1)}, bf16[384,512]{1,0:T(8,128)(2,1)S(1)}, u32[]{:S(2)}, u32[]{:S(2)}) collective-permute-start(bf16[384,512]{1,0:T(8,128)(2,1)S(1)} %reshape.114.own), channel_id=1, source_target_pairs={{0,3},{1,0},{2,1},{3,2},{4,7},{5,4},{6,5},{7,6},{8,11},{9,8},{10,9... | collective-permute-start | bytes 1179656 | tf_op jit(solution)/shard_map/ppermute | solution.py:27
  105.9 11.3 %collective-permute-start.19 = (bf16[384,512]{1,0:T(8,128)(2,1)S(1)}, bf16[384,512]{1,0:T(8,128)(2,1)S(1)}, u32[]{:S(2)}, u32[]{:S(2)}) collective-permute-start(bf16[384,512]{1,0:T(8,128)(2,1)S(1)} %reshape.114.own), channel_id=1, source_target_pairs={{0,1},{1,2},{2,3},{3,0},{4,5},{5,6},{6,7},{7,4},{8,9},{9,10},{10,1... | collective-permute-start | bytes 1179656 | tf_op jit(solution)/shard_map/ppermute | solution.py:27
  107.4 25.0 %copy-start.1 = (f32[2048]{0:T(1024)S(1)}, f32[2048]{0:T(1024)}, u32[]{:S(2)}) copy-start(f32[2048]{0:T(1024)} %param.21) | copy-start | bytes 24580
  107.8 19.1 %collective-permute-start.12 = (bf16[512,512]{1,0:T(8,128)(2,1)S(1)}, bf16[512,512]{1,0:T(8,128)(2,1)S(1)}, u32[]{:S(2)}, u32[]{:S(2)}) collective-permute-start(bf16[512,512]{1,0:T(8,128)(2,1)S(1)} %reshape.110.own), channel_id=1, source_target_pairs={{0,3},{1,0},{2,1},{3,2},{4,7},{5,4},{6,5},{7,6},{8,11},{9,8},{10,9... | collective-permute-start | bytes 1572872 | tf_op jit(solution)/shard_map/ppermute | solution.py:27
  109.1 19.4 %collective-permute-start.11 = (bf16[512,512]{1,0:T(8,128)(2,1)S(1)}, bf16[512,512]{1,0:T(8,128)(2,1)S(1)}, u32[]{:S(2)}, u32[]{:S(2)}) collective-permute-start(bf16[512,512]{1,0:T(8,128)(2,1)S(1)} %reshape.110.own), channel_id=1, source_target_pairs={{0,1},{1,2},{2,3},{3,0},{4,5},{5,6},{6,7},{7,4},{8,9},{9,10},{10,1... | collective-permute-start | bytes 1572872 | tf_op jit(solution)/shard_map/ppermute | solution.py:27
  115.7 15.4 %collective-permute-start.22 = (bf16[192,512]{1,0:T(8,128)(2,1)S(1)}, bf16[192,512]{1,0:T(8,128)(2,1)S(1)}, u32[]{:S(2)}, u32[]{:S(2)}) collective-permute-start(bf16[192,512]{1,0:T(8,128)(2,1)S(1)} %slice.75), channel_id=1, source_target_pairs={{0,3},{1,0},{2,1},{3,2},{4,7},{5,4},{6,5},{7,6},{8,11},{9,8},{10,9... | collective-permute-start | bytes 589832 | tf_op jit(solution)/shard_map/ppermute | solution.py:27
  117.3 15.1 %collective-permute-start.21 = (bf16[192,512]{1,0:T(8,128)(2,1)S(1)}, bf16[192,512]{1,0:T(8,128)(2,1)S(1)}, u32[]{:S(2)}, u32[]{:S(2)}) collective-permute-start(bf16[192,512]{1,0:T(8,128)(2,1)S(1)} %slice.74), channel_id=1, source_target_pairs={{0,1},{1,2},{2,3},{3,0},{4,5},{5,6},{6,7},{7,4},{8,9},{9,10},{10,1... | collective-permute-start | bytes 589832 | tf_op jit(solution)/shard_map/ppermute | solution.py:27
  126.9 16.9 %collective-permute-start.14 = (bf16[256,512]{1,0:T(8,128)(2,1)S(1)}, bf16[256,512]{1,0:T(8,128)(2,1)S(1)}, u32[]{:S(2)}, u32[]{:S(2)}) collective-permute-start(bf16[256,512]{1,0:T(8,128)(2,1)S(1)} %slice.72), channel_id=1, source_target_pairs={{0,3},{1,0},{2,1},{3,2},{4,7},{5,4},{6,5},{7,6},{8,11},{9,8},{10,9... | collective-permute-start | bytes 786440 | tf_op jit(solution)/shard_map/ppermute | solution.py:27
  128.5 15.3 %collective-permute-start.13 = (bf16[256,512]{1,0:T(8,128)(2,1)S(1)}, bf16[256,512]{1,0:T(8,128)(2,1)S(1)}, u32[]{:S(2)}, u32[]{:S(2)}) collective-permute-start(bf16[256,512]{1,0:T(8,128)(2,1)S(1)} %slice.71), channel_id=1, source_target_pairs={{0,1},{1,2},{2,3},{3,0},{4,5},{5,6},{6,7},{7,4},{8,9},{9,10},{10,1... | collective-permute-start | bytes 786440 | tf_op jit(solution)/shard_map/ppermute | solution.py:27
  141.1 16.1 %collective-permute-start.23 = (bf16[192,512]{1,0:T(8,128)(2,1)S(1)}, bf16[192,512]{1,0:T(8,128)(2,1)S(1)}, u32[]{:S(2)}, u32[]{:S(2)}) collective-permute-start(bf16[192,512]{1,0:T(8,128)(2,1)S(1)} %get-tuple-element.32), channel_id=1, source_target_pairs={{0,1},{1,2},{2,3},{3,0},{4,5},{5,6},{6,7},{7,4},{8,9},{9,10},{10,1... | collective-permute-start | bytes 589832 | tf_op jit(solution)/shard_map/ppermute | solution.py:27
  141.2 15.9 %collective-permute-start.25 = (bf16[192,512]{1,0:T(8,128)(2,1)S(1)}, bf16[192,512]{1,0:T(8,128)(2,1)S(1)}, u32[]{:S(2)}, u32[]{:S(2)}) collective-permute-start(bf16[192,512]{1,0:T(8,128)(2,1)S(1)} %get-tuple-element.34), channel_id=1, source_target_pairs={{0,3},{1,0},{2,1},{3,2},{4,7},{5,4},{6,5},{7,6},{8,11},{9,8},{10,9... | collective-permute-start | bytes 589832 | tf_op jit(solution)/shard_map/ppermute | solution.py:27
  154.3 9.4 %collective-permute-start.15 = (bf16[256,512]{1,0:T(8,128)(2,1)S(1)}, bf16[256,512]{1,0:T(8,128)(2,1)S(1)}, u32[]{:S(2)}, u32[]{:S(2)}) collective-permute-start(bf16[256,512]{1,0:T(8,128)(2,1)S(1)} %get-tuple-element.27), channel_id=1, source_target_pairs={{0,1},{1,2},{2,3},{3,0},{4,5},{5,6},{6,7},{7,4},{8,9},{9,10},{10,1... | collective-permute-start | bytes 786440 | tf_op jit(solution)/shard_map/ppermute | solution.py:27
  154.4 6.0 %collective-permute-start.17 = (bf16[256,512]{1,0:T(8,128)(2,1)S(1)}, bf16[256,512]{1,0:T(8,128)(2,1)S(1)}, u32[]{:S(2)}, u32[]{:S(2)}) collective-permute-start(bf16[256,512]{1,0:T(8,128)(2,1)S(1)} %get-tuple-element.29), channel_id=1, source_target_pairs={{0,3},{1,0},{2,1},{3,2},{4,7},{5,4},{6,5},{7,6},{8,11},{9,8},{10,9... | collective-permute-start | bytes 786440 | tf_op jit(solution)/shard_map/ppermute | solution.py:27
  157.2 10.1 %collective-permute-start.26 = (bf16[384,512]{1,0:T(8,128)(2,1)S(1)}, bf16[384,512]{1,0:T(8,128)(2,1)S(1)}, u32[]{:S(2)}, u32[]{:S(2)}) collective-permute-start(bf16[384,512]{1,0:T(8,128)(2,1)S(1)} %fusion.35), channel_id=1, source_target_pairs={{0,3},{1,0},{2,1},{3,2},{4,7},{5,4},{6,5},{7,6},{8,11},{9,8},{10,9... | collective-permute-start | bytes 1179656 | tf_op jit(solution)/shard_map/ppermute | solution.py:27
  157.3 11.3 %collective-permute-start.24 = (bf16[384,512]{1,0:T(8,128)(2,1)S(1)}, bf16[384,512]{1,0:T(8,128)(2,1)S(1)}, u32[]{:S(2)}, u32[]{:S(2)}) collective-permute-start(bf16[384,512]{1,0:T(8,128)(2,1)S(1)} %fusion.34), channel_id=1, source_target_pairs={{0,1},{1,2},{2,3},{3,0},{4,5},{5,6},{6,7},{7,4},{8,9},{9,10},{10,1... | collective-permute-start | bytes 1179656 | tf_op jit(solution)/shard_map/ppermute | solution.py:27
  160.5 22.5 %collective-permute-start.18 = (bf16[512,512]{1,0:T(8,128)(2,1)S(1)}, bf16[512,512]{1,0:T(8,128)(2,1)S(1)}, u32[]{:S(2)}, u32[]{:S(2)}) collective-permute-start(bf16[512,512]{1,0:T(8,128)(2,1)S(1)} %fusion.30), channel_id=1, source_target_pairs={{0,3},{1,0},{2,1},{3,2},{4,7},{5,4},{6,5},{7,6},{8,11},{9,8},{10,9... | collective-permute-start | bytes 1572872 | tf_op jit(solution)/shard_map/ppermute | solution.py:27
  163.8 19.3 %collective-permute-start.16 = (bf16[512,512]{1,0:T(8,128)(2,1)S(1)}, bf16[512,512]{1,0:T(8,128)(2,1)}, u32[]{:S(2)}, u32[]{:S(2)}) collective-permute-start(bf16[512,512]{1,0:T(8,128)(2,1)S(1)} %fusion.29), channel_id=1, source_target_pairs={{0,1},{1,2},{2,3},{3,0},{4,5},{5,6},{6,7},{7,4},{8,9},{9,10},{10,1... | collective-permute-start | bytes 1572872 | tf_op jit(solution)/shard_map/ppermute | solution.py:27
  169.8 28.4 %all-to-all-start.2 = ((bf16[64,24,128]{2,1,0:T(8,128)(2,1)}), bf16[64,24,128]{2,1,0:T(8,128)(2,1)S(1)}, u32[]{:S(2)}, u32[]{:S(2)}) async-start(bf16[64,24,128]{2,1,0:T(8,128)(2,1)} %reshape.115), calls=%async_computation.2 | async-start | bytes 786432 | tf_op jit(solution)/shard_map/all_to_all | solution.py:349
  183.0 20.6 %copy-start.10 = (f32[320,2]{0,1:T(2,128)S(1)}, f32[320,2]{0,1:T(2,128)}, u32[]{:S(2)}) copy-start(f32[320,2]{0,1:T(2,128)} %param.23) | copy-start | bytes 7684
  198.2 23.1 %all-to-all-start.1 = ((bf16[64,8,512]{2,1,0:T(8,128)(2,1)}), bf16[64,8,512]{2,1,0:T(8,128)(2,1)S(1)}, u32[]{:S(2)}, u32[]{:S(2)}) async-start(bf16[64,8,512]{2,1,0:T(8,128)(2,1)} %fusion.22), calls=%async_computation.1 | async-start | bytes 1048576 | tf_op jit(solution)/shard_map/all_to_all | solution.py:349
  (9 other events, 111.3 us)
